TPU v7x, 32 devices: a whole 2x2x4 slice. The times are simulated.
32 devices in a mesh: ep: 8 (over z, core), tp: 4 (over y, x).
Axes of the slice: x: 2, y: 2, z: 4, core: 2. Of those that a mesh axis runs over, the one named last changes fastest.
Arguments:
- mix_in: bfloat16 [2048, 2048], P('ep'), may hold values from -6 to 6
- mix_gain: float32 [2048], replicated, may hold values from 0.1 to 1.9
- w_in_x: bfloat16 [2048, 2048], P(None, 'tp'), may hold values from -0.125 to 0.125
- w_in_y: bfloat16 [2048, 2048], P(None, 'tp'), may hold values from -0.125 to 0.125
- conv_taps: float32 [4, 2048], P(None, 'tp'), may hold values from -3 to 3
- recur_gate_w: bfloat16 [16, 128, 128], P('tp'), may hold values from -0.5 to 0.5
- input_gate_w: bfloat16 [16, 128, 128], P('tp'), may hold values from -0.5 to 0.5
- decay_logit: float32 [2048], P('tp'), may hold values from 4 to 20
- decay_shift: float32 [2048, 2048], P('ep', 'tp'), may hold values from -2.2 to 0
- moe_in: bfloat16 [2048, 2048], P('ep'), may hold values from -6 to 6
- moe_gain: float32 [2048], replicated, may hold values from 0.1 to 1.9
- routes: int32 [2048, 2], P('ep'), may hold values from 0 to 7, all different within a row; in each aligned block of 256 rows (0 to 255, 256 to 511, ...) at most 128 rows name the same one
- route_weight: float32 [2048, 2], P('ep'), may hold values from 0.1 to 1
- expert_gate: bfloat16 [8, 2048, 2048], P('ep', None, 'tp'), may hold values from -0.125 to 0.125
- expert_up: bfloat16 [8, 2048, 2048], P('ep', None, 'tp'), may hold values from -0.125 to 0.125
- expert_down: bfloat16 [8, 2048, 2048], P('ep', None, 'tp'), may hold values from -0.125 to 0.125
Outputs:
- mixer_out: bfloat16 [2048, 2048], P('ep', 'tp')
- moe_out: bfloat16 [2048, 2048], P('ep', 'tp')
Inputs may be any that keep to these rules, and one draw needn't show every extreme that they name: `routes`: each row names 2 different experts. Among the rows of one index of ep no expert is named more than 128 times, a bound that some block reaches.
All inputs are finite; a program needn't handle non-finite values.
Results may differ from a plain program's by a relative error of at most 0.0095.
Values may be sent and summed in bfloat16 or wider, within the bound.
A program may use at most 64 MiB of HBM per device.

v0:
```python
import functools

import jax
import jax.numpy as jnp
from jax import lax
from jax.experimental import pallas as pl
from jax.experimental.pallas import tpu as pltpu
from jax.sharding import PartitionSpec as P

epsilon = 1e-06
lru_scale = 8.0
MESH = pl.DeviceIdType.MESH
F32 = jnp.float32
BF16 = jnp.bfloat16


block_order = ((0, 2, 3, 1), (1, 2, 3, 0), (2, 1, 0, 3), (3, 1, 0, 2))


def one_minus_exp(value):
    series = jnp.full_like(value, 1.0 / 9.0)
    for k in range(8, 1, -1):
        series = (1.0 + value * series) * (1.0 / k)
    series = 1.0 + value * series
    return jnp.where(value > -0.5, -value * series, 1.0 - jnp.exp(value))


def both_kernel(
    cap,
    mix_hbm,
    wx_hbm,
    wy_hbm,
    ga_hbm,
    gx_hbm,
    shift_hbm,
    mix_gain_ref,
    taps_ref,
    soft_ref,
    moe_hbm,
    gain_ref,
    rt_row,
    rw_row,
    gate_hbm,
    up_hbm,
    down_hbm,
    mix_ref,
    out_ref,
    tok,
    hid,
    xs,
    res,
    ret,
    routes_all,
    gw,
    uw,
    dw,
    load_sem,
    rt_sem,
    z_send,
    z_recv,
    t_sem,
    sib_sem,
    own_sem,
    h_sem,
    ret_sem,
    mixv,
    wx,
    wy,
    gaw,
    gxw,
    shiftv,
    xb,
    yb,
    av,
    bv,
    ends,
    halo_sem,
    ends_sem,
):
    n_ep = lax.axis_size("ep")
    nz = n_ep // 2
    ep = lax.axis_index("ep")
    t = lax.axis_index("tp")
    z, c = ep // 2, ep % 2
    y, x = t // 2, t % 2
    xp, yp, dg = y * 2 + (1 - x), (1 - y) * 2 + x, 3 - t
    rows, share = tok.shape[3], tok.shape[4]
    half = rows // 2
    pair = 2 * cap
    pair_half = pair // 2
    sibling = {"ep": z * 2 + (1 - c)}
    table = block_order

    def block_at(s):
        q = jnp.int32(0)
        for zz in range(nz):
            for ss in range(nz):
                q = jnp.where((z == zz) & (s == ss), table[zz][ss], q)
        return q

    def remote(src, dst, send, recv, where):
        return pltpu.make_async_remote_copy(
            src_ref=src,
            dst_ref=dst,
            send_sem=send,
            recv_sem=recv,
            device_id=where,
            device_id_type=MESH,
        )

    loads = [
        pltpu.make_async_copy(
            moe_hbm.at[:, pl.ds(k * share, share)], tok.at[c, z, k], load_sem.at[k]
        )
        for k in range(4)
    ] + [
        pltpu.make_async_copy(gate_hbm.at[0], gw, load_sem.at[4]),
        pltpu.make_async_copy(up_hbm.at[0], uw, load_sem.at[5]),
        pltpu.make_async_copy(mix_hbm, mixv, load_sem.at[6]),
        pltpu.make_async_copy(wx_hbm, wx, load_sem.at[7]),
        pltpu.make_async_copy(wy_hbm, wy, load_sem.at[8]),
        pltpu.make_async_copy(ga_hbm, gaw, load_sem.at[9]),
        pltpu.make_async_copy(gx_hbm, gxw, load_sem.at[10]),
        pltpu.make_async_copy(shift_hbm, shiftv, load_sem.at[11]),
        pltpu.make_async_copy(down_hbm.at[0], dw, load_sem.at[12]),
    ]
    for copy in loads:
        copy.start()

    barrier = pltpu.get_barrier_semaphore()
    for by in range(1, n_ep):
        pl.semaphore_signal(
            barrier, inc=1, device_id={"ep": (ep + by) % n_ep}, device_id_type=MESH
        )
    for peer in (xp, yp):
        pl.semaphore_signal(barrier, inc=1, device_id={"tp": peer}, device_id_type=MESH)
    pl.semaphore_wait(barrier, n_ep + 1)

    def route_copy(by):
        return remote(
            rt_row,
            routes_all.at[ep],
            rt_sem.at[0, by],
            rt_sem.at[1, ep],
            {"ep": (ep + by) % n_ep},
        )

    for by in range(1, n_ep):
        route_copy(by).start()
    routes_all[ep] = rt_row[...]

    def z_copy(q, up):
        return remote(
            tok.at[c, q, t],
            tok.at[c, q, t],
            z_send.at[up, q],
            z_recv.at[q],
            {"ep": ep + (2 if up else -2)},
        )

    def t_copy(q, kind):
        owner = (t, t, t, t, yp, xp)[kind]
        start = (0, half, half, 0, half, 0)[kind]
        part = tok.at[c, q, owner, pl.ds(start, half)]
        where = {"tp": (xp, yp)[kind % 2]}
        return remote(part, part, t_sem.at[0, kind, q], t_sem.at[1, kind, q], where)

    def sib_copy(q, k):
        part = tok.at[c, q, k]
        return remote(part, part, sib_sem.at[0, k, q], sib_sem.at[1, k, q], sibling)

    def own_copy():
        part = tok.at[c, z]
        return remote(part, part, own_sem.at[0], own_sem.at[1], sibling)

    def h_copy(q, kind):
        owner = (t, t, t, t, yp, xp)[kind]
        start = (0, pair_half, pair_half, 0, pair_half, 0)[kind]
        part = hid.at[q, owner, pl.ds(start, pair_half)]
        where = {"tp": (xp, yp)[kind % 2]}
        return remote(part, part, h_sem.at[0, kind, q], h_sem.at[1, kind, q], where)

    def ret_copy(q, cc):
        part = res.at[q * 2 + cc]
        return remote(
            part, ret.at[ep], ret_sem.at[0, q * 2 + cc], ret_sem.at[1, ep], {"ep": q * 2 + cc}
        )

    def spread(q):
        for kind in range(4):
            t_copy(q, kind).start()
        sib_copy(q, t).start()

    def arrive(q):
        z_copy(q, 1).wait_recv()

        @pl.when((q < z) & (z + 1 < nz))
        def _():
            z_copy(q, 1).start()

        @pl.when((q > z) & (z > 0))
        def _():
            z_copy(q, 0).start()

    def ranks_row(block):
        named = routes_all[block]
        mask = jnp.where((named[0:1] == ep) | (named[1:2] == ep), 1.0, 0.0)
        before = jnp.where(
            lax.broadcasted_iota(jnp.int32, (rows, rows), 0)
            < lax.broadcasted_iota(jnp.int32, (rows, rows), 1),
            1.0,
            0.0,
        ).astype(BF16)
        rank = jnp.dot(
            jnp.broadcast_to(mask, (8, rows)).astype(BF16), before, preferred_element_type=F32
        )[0:1]
        key = jnp.where(mask > 0.5, rank, -1.0)
        seat = lax.broadcasted_iota(jnp.int32, (cap, rows), 0).astype(F32)
        return jnp.where(seat == key, 1.0, 0.0).astype(BF16)

    def expert_in(q):
        for cc in range(2):
            pick = ranks_row(q * 2 + cc)
            parts = [
                jnp.dot(pick, tok[cc, q, k], preferred_element_type=F32) for k in range(4)
            ]
            square = sum(jnp.sum(part * part, axis=-1, keepdims=True) for part in parts)
            scale = lax.rsqrt(square * (1.0 / (4 * share)) + epsilon)
            for k in range(4):
                xs[pl.ds(cc * cap, cap), pl.ds(k * share, share)] = (
                    parts[k] * scale * gain_ref[:, pl.ds(k * share, share)]
                ).astype(BF16)

        tile = 256

        @pl.loop(0, gw.shape[1] // tile)
        def _(j):
            cols = pl.ds(pl.multiple_of(j * tile, tile), tile)
            g = jnp.dot(xs[...], gw[:, cols], preferred_element_type=F32)
            u = jnp.dot(xs[...], uw[:, cols], preferred_element_type=F32)
            hid[q, t, :, cols] = (jax.nn.silu(g) * u).astype(BF16)

        for kind in range(4):
            h_copy(q, kind).start()

    def expert_out(q):
        tile = 256
        span = hid.shape[3]

        @pl.loop(0, dw.shape[1] // tile)
        def _(j):
            cols = pl.ds(pl.multiple_of(j * tile, tile), tile)
            total = jnp.zeros((pair, tile), F32)
            for k in range(4):
                total = total + jnp.dot(
                    hid[q, k], dw[pl.ds(k * span, span), cols], preferred_element_type=F32
                )
            out = total.astype(BF16)
            res[q * 2, :, cols] = out[:cap]
            res[q * 2 + 1, :, cols] = out[cap:]

        for cc in range(2):
            mine = (q == z) & (c == cc)

            @pl.when(jnp.logical_not(mine))
            def _():
                ret_copy(q, cc).start()

            @pl.when(mine)
            def _():
                ret[ep] = res[q * 2 + cc]

    pad = xb.shape[0] - rows

    def halo_copy():
        return remote(
            xb.at[pl.ds(rows, pad)],
            xb.at[pl.ds(0, pad)],
            halo_sem.at[0],
            halo_sem.at[1],
            {"ep": ep + 1},
        )

    def ends_copy(by):
        return remote(
            ends.at[ep],
            ends.at[ep],
            ends_sem.at[0, by],
            ends_sem.at[1, ep],
            {"ep": (ep + by) % n_ep},
        )

    def project():
        for k in range(6, 9):
            loads[k].wait()
        strip = 64

        @pl.loop(0, rows // strip)
        def _(i):
            at = pl.ds(pl.multiple_of(i * strip, strip), strip)
            wide = mixv[at, :].astype(F32)
            scale = lax.rsqrt(jnp.mean(wide * wide, axis=-1, keepdims=True) + epsilon)
            xs[at, :] = (wide * scale * mix_gain_ref[...]).astype(BF16)

        tile = 256

        @pl.loop(0, wx.shape[1] // tile)
        def _(j):
            cols = pl.ds(pl.multiple_of(j * tile, tile), tile)
            xb[pl.ds(pad, rows), cols] = jnp.dot(
                xs[...], wx[:, cols], preferred_element_type=F32
            ).astype(BF16)
            yb[:, cols] = jnp.dot(xs[...], wy[:, cols], preferred_element_type=F32).astype(BF16)

        @pl.when(ep + 1 < n_ep)
        def _():
            halo_copy().start()

        @pl.when(ep == 0)
        def _():
            xb[pl.ds(0, pad), :] = jnp.zeros((pad, xb.shape[1]), BF16)

    def drives():
        for k in range(9, 12):
            loads[k].wait()

        @pl.when(ep > 0)
        def _():
            halo_copy().wait_recv()

        taps = taps_ref.shape[0]
        size = gaw.shape[1]
        for h in range(gaw.shape[0]):
            cols = pl.ds(h * size, size)
            wide = xb[:, cols].astype(F32)
            conv = jnp.zeros((rows, size), F32)
            for k in range(taps):
                first_row = pad - (taps - 1) + k
                conv = conv + taps_ref[k : k + 1, cols] * wide[first_row : first_row + rows]
            x_conv = conv.astype(BF16)
            gate_a = jnp.dot(x_conv, gaw[h], preferred_element_type=F32)
            gate_x = jnp.dot(x_conv, gxw[h], preferred_element_type=F32)
            log_decay = (
                -lru_scale * jax.nn.sigmoid(gate_a) * soft_ref[:, cols] + shiftv[:, cols]
            )
            av[:, cols] = jnp.exp(log_decay)
            bv[:, cols] = (
                jnp.sqrt(one_minus_exp(2.0 * log_decay))
                * jax.nn.sigmoid(gate_x)
                * x_conv.astype(F32)
            )

    def recur():
        width = av.shape[1]
        row = lax.broadcasted_iota(jnp.int32, (8, width), 0)

        def group(i, carry):
            at = pl.ds(pl.multiple_of(i * 8, 8), 8)
            a, b = av[at, :], bv[at, :]
            for by in (1, 2, 4):
                a_past, b_past = pltpu.roll(a, by, 0), pltpu.roll(b, by, 0)
                b = jnp.where(row >= by, a * b_past + b, b)
                a = jnp.where(row >= by, a * a_past, a)
            b = a * carry[1] + b
            a = a * carry[0]
            av[at, :] = a
            bv[at, :] = b
            return (a[7:8], b[7:8])

        through, state = lax.fori_loop(
            0, rows // 8, group, (jnp.ones((1, width), F32), jnp.zeros((1, width), F32))
        )
        ends[ep, 0:1] = through
        ends[ep, 1:2] = state
        for by in range(1, n_ep):
            ends_copy(by).start()

    def finish():
        carried = jnp.zeros((1, av.shape[1]), F32)
        for by in range(1, n_ep):
            other = (ep + by) % n_ep
            remote(
                ends.at[other], ends.at[other], ends_sem.at[0, 0], ends_sem.at[1, other], {"ep": other}
            ).wait_recv()
        for k in range(n_ep):
            entered = ends[k, 0:1] * carried + ends[k, 1:2]
            carried = jnp.where(k < ep, entered, carried)
        strip = 32

        @pl.loop(0, rows // strip)
        def _(i):
            at = pl.ds(pl.multiple_of(i * strip, strip), strip)
            state = bv[at, :] + av[at, :] * carried
            mix_ref[at, :] = (state * jax.nn.gelu(yb[at, :].astype(F32))).astype(BF16)

    for k in range(4):
        loads[k].wait()

    @pl.when(z + 1 < nz)
    def _():
        z_copy(z, 1).start()

    @pl.when(z > 0)
    def _():
        z_copy(z, 0).start()

    own_copy().start()
    for k in range(4, 6):
        loads[k].wait()
    for by in range(1, n_ep):
        other = (ep + by) % n_ep
        remote(
            rt_row, routes_all.at[other], rt_sem.at[0, 0], rt_sem.at[1, other], {"ep": other}
        ).wait_recv()
    remote(
        tok.at[1 - c, z], tok.at[1 - c, z], own_sem.at[0], own_sem.at[1], sibling
    ).wait_recv()
    expert_in(z)
    first = block_at(1)

    @pl.when(z > 0)
    def _():
        arrive(z - 1)

    @pl.when(z + 1 < nz)
    def _():
        arrive(z + 1)

    @pl.when((first == z + 2) | (first == z - 2))
    def _():
        arrive(first)

    spread(first)

    def pass_hidden(q):
        h_copy(q, 0).wait_recv()
        h_copy(q, 5).start()
        h_copy(q, 1).wait_recv()
        h_copy(q, 4).start()

    project()
    pass_hidden(z)
    loads[12].wait()

    @pl.when((z > 0) & (z + 1 < nz))
    def _():
        arrive(jnp.where(z + 2 < nz, z + 2, z - 2))

    def step(s, carry):
        q = block_at(s)
        nxt = block_at(s + 1)
        far = block_at(s + 2)

        @pl.when(s + 1 == nz)
        def _():
            pass_hidden(q)

        @pl.when(s + 1 < nz)
        def _():
            t_copy(nxt, 0).wait_recv()
            t_copy(nxt, 5).start()
            t_copy(nxt, 1).wait_recv()
            t_copy(nxt, 4).start()

            @pl.when(s + 2 < nz)
            def _():
                @pl.when((far == z + 3) | (far == z - 3))
                def _():
                    arrive(far)

                spread(far)

            @pl.when(s > 0)
            def _():
                pass_hidden(q)

            t_copy(nxt, 2).wait_recv()
            sib_copy(nxt, xp).start()
            t_copy(nxt, 3).wait_recv()
            sib_copy(nxt, yp).start()
            t_copy(nxt, 4).wait_recv()
            t_copy(nxt, 5).wait_recv()
            sib_copy(nxt, dg).start()
            for k in range(4):
                sib_copy(nxt, k).wait_recv()
            expert_in(nxt)

        for kind in range(2, 6):
            h_copy(q, kind).wait_recv()
        expert_out(q)

        @pl.when(s == 0)
        def _():
            drives()

        @pl.when(s == 1)
        def _():
            recur()

        @pl.when(s == 2)
        def _():
            finish()

        return carry

    lax.fori_loop(0, nz, step, 0)

    weights = rw_row[...]
    columns = jnp.concatenate(
        [
            rt_row[...].astype(F32),
            weights / (weights[0:1] + weights[1:2]),
            jnp.zeros((124, rows), F32),
        ],
        axis=0,
    ).T
    one, two = columns[:, 0:1].astype(jnp.int32), columns[:, 1:2].astype(jnp.int32)
    lane = lax.broadcasted_iota(jnp.int32, (rows, 128), 1)
    mask = jnp.where((one == lane) | (two == lane), 1.0, 0.0)
    before = jnp.where(
        lax.broadcasted_iota(jnp.int32, (rows, rows), 1)
        < lax.broadcasted_iota(jnp.int32, (rows, rows), 0),
        1.0,
        0.0,
    ).astype(BF16)
    rank = jnp.dot(before, mask.astype(BF16), preferred_element_type=F32)
    key = jnp.where(mask > 0.5, rank, -1.0)
    part_one, part_two = columns[:, 2:3], columns[:, 3:4]
    seat = lax.broadcasted_iota(jnp.int32, (rows, cap), 1).astype(F32)
    for by in range(1, n_ep):
        other = (ep + by) % n_ep
        remote(
            res.at[other], ret.at[other], ret_sem.at[0, other], ret_sem.at[1, other], {"ep": other}
        ).wait_recv()
    total = jnp.zeros((rows, ret.shape[2]), F32)
    for e in range(n_ep):
        pick = jnp.where(seat == key[:, e : e + 1], 1.0, 0.0).astype(BF16)
        portion = jnp.where(one == e, part_one, 0.0) + jnp.where(two == e, part_two, 0.0)
        total = total + portion * jnp.dot(pick, ret[e], preferred_element_type=F32)
    out_ref[...] = total.astype(BF16)

    for by in range(1, n_ep):
        route_copy(by).wait_send()

    @pl.when(z + 1 < nz)
    def _():
        z_copy(z, 1).wait_send()

    @pl.when(z > 0)
    def _():
        z_copy(z, 0).wait_send()

    own_copy().wait_send()

    @pl.when(ep + 1 < n_ep)
    def _():
        halo_copy().wait_send()

    for by in range(1, n_ep):
        ends_copy(by).wait_send()

    def drain(q, carry):
        for kind in range(6):
            h_copy(q, kind).wait_send()

        @pl.when(q != z)
        def _():
            for kind in range(6):
                t_copy(q, kind).wait_send()
            for k in range(4):
                sib_copy(q, k).wait_send()

        @pl.when((q < z) & (z + 1 < nz))
        def _():
            z_copy(q, 1).wait_send()

        @pl.when((q > z) & (z > 0))
        def _():
            z_copy(q, 0).wait_send()

        for cc in range(2):

            @pl.when((q != z) | (c != cc))
            def _():
                ret_copy(q, cc).wait_send()

        return carry

    lax.fori_loop(0, nz, drain, 0)


def both_fused(
    mix_in,
    mix_gain,
    w_in_x,
    w_in_y,
    conv_taps,
    recur_gate_w,
    input_gate_w,
    decay_logit,
    decay_shift,
    moe_in,
    moe_gain,
    routes,
    route_weight,
    expert_gate,
    expert_up,
    expert_down,
):
    n_ep = lax.axis_size("ep")
    nz = n_ep // 2
    rows, features = moe_in.shape
    share = features // 4
    ff_dev, out_dev = expert_gate.shape[2], expert_down.shape[2]
    width = w_in_x.shape[1]
    cap = 2 * rows * routes.shape[1] // n_ep
    vmem = pl.BlockSpec(memory_space=pltpu.VMEM)
    hbm = pl.BlockSpec(memory_space=pltpu.HBM)
    dma = pltpu.SemaphoreType.DMA
    flops = 2 * n_ep * cap * features * (2 * ff_dev + out_dev)
    return pl.pallas_call(
        functools.partial(both_kernel, cap),
        out_shape=(
            jax.ShapeDtypeStruct((rows, width), BF16),
            jax.ShapeDtypeStruct((rows, out_dev), BF16),
        ),
        in_specs=[hbm] * 6 + [vmem] * 3 + [hbm] + [vmem] * 3 + [hbm] * 3,
        out_specs=(vmem, vmem),
        scratch_shapes=[
            pltpu.VMEM((2, nz, 4, rows, share), BF16),
            pltpu.VMEM((nz, 4, 2 * cap, ff_dev), BF16),
            pltpu.VMEM((2 * cap, features), BF16),
            pltpu.VMEM((n_ep, cap, out_dev), BF16),
            pltpu.VMEM((n_ep, cap, out_dev), BF16),
            pltpu.VMEM((n_ep, 2, rows), jnp.int32),
            pltpu.VMEM(expert_gate.shape[1:], BF16),
            pltpu.VMEM(expert_up.shape[1:], BF16),
            pltpu.VMEM(expert_down.shape[1:], BF16),
            dma((13,)),
            dma((2, n_ep)),
            dma((2, nz)),
            dma((nz,)),
            dma((2, 6, nz)),
            dma((2, 4, nz)),
            dma((2,)),
            dma((2, 6, nz)),
            dma((2, n_ep)),
            pltpu.VMEM(mix_in.shape, BF16),
            pltpu.VMEM(w_in_x.shape, BF16),
            pltpu.VMEM(w_in_y.shape, BF16),
            pltpu.VMEM(recur_gate_w.shape, BF16),
            pltpu.VMEM(input_gate_w.shape, BF16),
            pltpu.VMEM((rows, width), F32),
            pltpu.VMEM((16 + rows, width), BF16),
            pltpu.VMEM((rows, width), BF16),
            pltpu.VMEM((rows, width), F32),
            pltpu.VMEM((rows, width), F32),
            pltpu.VMEM((n_ep, 2, width), F32),
            dma((2,)),
            dma((2, n_ep)),
        ],
        compiler_params=pltpu.CompilerParams(
            collective_id=0, has_side_effects=True, vmem_limit_bytes=60 * 1024 * 1024
        ),
        cost_estimate=pl.CostEstimate(flops=flops, bytes_accessed=16 << 20, transcendentals=0),
        name="both",
    )(
        mix_in,
        w_in_x,
        w_in_y,
        recur_gate_w,
        input_gate_w,
        decay_shift,
        mix_gain[None, :],
        conv_taps,
        jax.nn.softplus(-decay_logit)[None, :],
        moe_in,
        moe_gain[None, :],
        routes.T,
        route_weight.T,
        expert_gate,
        expert_up,
        expert_down,
    )


def from_behind(value, axis, by):
    count = lax.axis_size(axis)
    pairs = [(i, i + by) for i in range(count) if 0 <= i + by < count]
    return lax.ppermute(value, axis, pairs)


def entering(value, axis, combine, identity):
    count, index = (lax.axis_size(axis), lax.axis_index(axis))
    everything = jax.tree.map(lambda part: lax.all_gather(part, axis), value)
    start = jax.tree.map(
        lambda part, zero: jnp.broadcast_to(jnp.asarray(zero, part.dtype), part.shape),
        value,
        identity,
    )

    def hop(k, before):
        reached = k < index
        new = combine(before, jax.tree.map(lambda part: part[k], everything))
        return jax.tree.map(lambda a, b: jnp.where(reached, a, b), new, before)

    return lax.fori_loop(0, count, hop, start)


def norm_rows(rows, gain):
    widened = rows.astype(jnp.float32)
    scaled = widened * lax.rsqrt(jnp.mean(widened * widened, axis=-1, keepdims=True) + epsilon)
    return (scaled * gain[None, :]).astype(jnp.bfloat16)


def link(earlier, later):
    return (earlier[0] * later[0], later[0] * earlier[1] + later[1])


def fits_fused(moe_in, routes):
    n_ep = lax.axis_size("ep")
    gathered = n_ep * moe_in.size * moe_in.dtype.itemsize
    even = n_ep == 4 * routes.shape[1] == 2 * len(block_order)
    return lax.axis_size("tp") == 4 and even and gathered <= (16 << 20)


def moe_staged(moe_in, moe_gain, routes, route_weight, expert_gate, expert_up, expert_down):
    moe_rows = norm_rows(moe_in, moe_gain)
    token_count = moe_rows.shape[0]
    feature_count = moe_rows.shape[1]
    choose_count = routes.shape[1]
    expert_count = lax.axis_size("ep")
    capacity = 2 * token_count * choose_count // expert_count
    slot_total = expert_count * capacity
    expert_ids = routes.reshape(-1)
    onehot = (expert_ids[:, None] == jnp.arange(expert_count, dtype=jnp.int32)[None, :]).astype(
        jnp.int32
    )
    slot_rank = jnp.sum(jnp.cumsum(onehot, axis=0) * onehot, axis=1) - 1
    slot_index = expert_ids * capacity + slot_rank
    token_index = jnp.repeat(jnp.arange(token_count, dtype=jnp.int32), choose_count)
    slot_owner = jnp.full((slot_total,), token_count, jnp.int32).at[slot_index].set(token_index)
    padded_rows = jnp.concatenate([moe_rows, jnp.zeros((1, feature_count), jnp.bfloat16)], axis=0)
    outgoing = padded_rows[slot_owner].reshape(expert_count, capacity, feature_count)
    column_width = feature_count // lax.axis_size("tp")
    own_columns = lax.dynamic_slice_in_dim(
        outgoing, lax.axis_index("tp") * column_width, column_width, 2
    )
    incoming = lax.all_to_all(own_columns, "ep", split_axis=0, concat_axis=0, tiled=True)
    piece = lax.all_gather(incoming, "tp", axis=2, tiled=True)
    flat_rows = piece.reshape(slot_total, piece.shape[2])
    gate_rows = expert_gate[0]
    up_rows = expert_up[0]
    gate_proj = jnp.dot(flat_rows, gate_rows, preferred_element_type=jnp.float32)
    up_proj = jnp.dot(flat_rows, up_rows, preferred_element_type=jnp.float32)
    hidden = (jax.nn.silu(gate_proj) * up_proj).astype(jnp.bfloat16)
    down_rows = expert_down[0]
    columns = jnp.dot(
        lax.all_gather(hidden, "tp", axis=1, tiled=True),
        down_rows,
        preferred_element_type=jnp.float32,
    )
    results = columns.astype(jnp.bfloat16).reshape(expert_count, capacity, expert_down.shape[2])
    returned = lax.all_to_all(results, "ep", split_axis=0, concat_axis=0, tiled=True).reshape(
        slot_total, expert_down.shape[2]
    )
    picked = (
        returned[slot_index]
        .astype(jnp.float32)
        .reshape(token_count, choose_count, expert_down.shape[2])
    )
    route_share = route_weight / jnp.sum(route_weight, axis=1, keepdims=True)
    moe_out = jnp.sum(route_share[:, :, None] * picked, axis=1).astype(jnp.bfloat16)
    return moe_out


def staged(
    mix_in,
    mix_gain,
    w_in_x,
    w_in_y,
    conv_taps,
    recur_gate_w,
    input_gate_w,
    decay_logit,
    decay_shift,
    moe_in,
    moe_gain,
    routes,
    route_weight,
    expert_gate,
    expert_up,
    expert_down,
):
    row_count = mix_in.shape[0]
    width_dev = w_in_x.shape[1]
    heads_dev = recur_gate_w.shape[0]
    block_size = recur_gate_w.shape[1]
    tap_count = conv_taps.shape[0]
    mixer_rows = norm_rows(mix_in, mix_gain)
    x_branch = jnp.dot(mixer_rows, w_in_x, preferred_element_type=jnp.float32).astype(jnp.bfloat16)
    y_branch = jnp.dot(mixer_rows, w_in_y, preferred_element_type=jnp.float32).astype(jnp.bfloat16)
    previous = from_behind(x_branch[row_count - (tap_count - 1) :], "ep", 1)
    padded = jnp.concatenate([previous, x_branch], axis=0)
    conv_sum = jnp.zeros((row_count, width_dev), jnp.float32)
    for tap_index in range(tap_count):
        conv_sum = conv_sum + conv_taps[tap_index][None, :] * padded[
            tap_index : tap_index + row_count
        ].astype(jnp.float32)
    x_conv = conv_sum.astype(jnp.bfloat16)
    heads_in = x_conv.reshape(row_count, heads_dev, block_size)
    gate_a = jnp.einsum(
        "thi,hij->thj", heads_in, recur_gate_w, preferred_element_type=jnp.float32
    ).reshape(row_count, width_dev)
    gate_x = jnp.einsum(
        "thi,hij->thj", heads_in, input_gate_w, preferred_element_type=jnp.float32
    ).reshape(row_count, width_dev)
    log_decay = (
        -lru_scale * jax.nn.sigmoid(gate_a) * jax.nn.softplus(-decay_logit)[None, :] + decay_shift
    )
    lru_drive = (
        jnp.sqrt(-jnp.expm1(2.0 * log_decay)) * jax.nn.sigmoid(gate_x) * x_conv.astype(jnp.float32)
    )
    through, local_state = lax.associative_scan(link, (jnp.exp(log_decay), lru_drive), axis=0)
    identity = (jnp.ones((width_dev,), jnp.float32), jnp.zeros((width_dev,), jnp.float32))
    carried = entering((through[row_count - 1], local_state[row_count - 1]), "ep", link, identity)
    lru_state = local_state + through * carried[1][None, :]
    mixer_out = (lru_state * jax.nn.gelu(y_branch.astype(jnp.float32))).astype(jnp.bfloat16)
    moe_out = moe_staged(
        moe_in, moe_gain, routes, route_weight, expert_gate, expert_up, expert_down
    )
    return (mixer_out, moe_out)


def local(*args):
    return (both_fused if fits_fused(args[9], args[11]) else staged)(*args)


def solution(mesh):
    placed = (
        P("ep", None),
        P(),
        P(None, "tp"),
        P(None, "tp"),
        P(None, "tp"),
        P("tp", None, None),
        P("tp", None, None),
        P("tp"),
        P("ep", "tp"),
        P("ep", None),
        P(),
        P("ep", None),
        P("ep", None),
        P("ep", None, "tp"),
        P("ep", None, "tp"),
        P("ep", None, "tp"),
    )
    return jax.shard_map(
        local, mesh=mesh, in_specs=placed, out_specs=(P("ep", "tp"), P("ep", "tp")), check_vma=False
    )
```

profile of v0, /device:TPU:1, one launch (start us, length us, event | category | flops | bytes accessed | tf_op | source)
XLA Modules:
  0.0 94.3 jit_solution(2718100735016470244)
XLA Ops:
  0.6 1.3 %compare_select_fusion = f32[512]{0:T(512)} fusion(f32[512]{0:T(512)} %param.23), kind=kLoop, calls=%fused_computation | loop fusion | flops 3584 | bytes 4096 | tf_op jit(solution)/shard_map/jit(softplus)/select_n | solution.py:676
  1.9 89.0 %both.1 = (bf16[256,512]{1,0:T(8,128)(2,1)}, bf16[256,512]{1,0:T(8,128)(2,1)}) custom-call(bf16[256,2048]{1,0:T(8,128)(2,1)} %mix_hbm.1, bf16[2048,512]{1,0:T(8,128)(2,1)} %wx_hbm.1, bf16[2048,512]{1,0:T(8,128)(2,1)} %wy_hbm.1, bf16[4,128,128]{2,1,0:T(8,128)(2,1)} %ga_hbm.1, bf16[4,128,128]{2,1,0:T(8,128)(2,1)} %gx_hbm.1, f32[256,512]{1,0:T(8,128)} %shift_hbm.1, ...), custom_call_target="tpu_custom_call" | custom-call | flops 6442450944 | bytes 16777216 | tf_op jit(solution)/shard_map/both/pallas_call | solution.py:621
  90.9 1.7 %copy.20 = bf16[256,512]{1,0:T(8,128)(2,1)} copy(bf16[256,512]{1,0:T(8,128)(2,1)} %get-tuple-element.4) | data formatting | bytes 524288
  92.6 1.7 %copy.21 = bf16[256,512]{1,0:T(8,128)(2,1)} copy(bf16[256,512]{1,0:T(8,128)(2,1)} %get-tuple-element.5) | data formatting | bytes 524288
where the time goes:
time: 94.5 us; the launch traced here: 94.3 us
  Pallas kernels  89 us (94%)
  local copies, waits for them, and re-layouts  3.34 us (4%)
  other arithmetic  1.28 us (1%)
    pallas_call x1, Pallas kernels, both_fused(): pl.pallas_call(functools.partial(both_kernel, cap), out_shape=(jax.ShapeD...  89 us
    unnamed x2, local copies, waits for them, and re-layouts  3.34 us

commit v1 on v0

v1 whole, which is shorter than its diff:
```python
import functools

import jax
import jax.numpy as jnp
from jax import lax
from jax.experimental import pallas as pl
from jax.experimental.pallas import tpu as pltpu
from jax.sharding import PartitionSpec as P

epsilon = 1e-06
lru_scale = 8.0
MESH = pl.DeviceIdType.MESH
F32 = jnp.float32
BF16 = jnp.bfloat16


block_order = ((1, 2, 3), (0, 3, 2), (3, 0, 1), (2, 1, 0))


def one_minus_exp(value):
    series = jnp.full_like(value, 1.0 / 9.0)
    for k in range(8, 1, -1):
        series = (1.0 + value * series) * (1.0 / k)
    series = 1.0 + value * series
    return jnp.where(value > -0.5, -value * series, 1.0 - jnp.exp(value))


def soft_plus(value):
    small = jnp.exp(-jnp.abs(value))
    series = jnp.full_like(small, 1.0 / 7.0)
    for k in range(6, 0, -1):
        series = 1.0 / k - small * series
    wide = jnp.where(small < 0.05, small * series, jnp.log(1.0 + small))
    return jnp.maximum(value, 0.0) + wide


def both_kernel(
    cap,
    mix_hbm,
    wx_hbm,
    wy_hbm,
    ga_hbm,
    gx_hbm,
    shift_hbm,
    mix_gain_ref,
    taps_ref,
    logit_ref,
    moe_hbm,
    gain_ref,
    rt_row,
    rw_row,
    gate_hbm,
    up_hbm,
    down_hbm,
    mix_ref,
    out_ref,
    nrm,
    tok,
    xs,
    stage,
    own_stage,
    picks,
    hid,
    psend,
    precv,
    pown,
    res,
    ret,
    routes_all,
    comb,
    part,
    total,
    gw,
    uw,
    w2,
    load_sem,
    rt_sem,
    z_send,
    z_recv,
    w_sem,
    x_send,
    x_recv,
    ag_sem,
    rs_sem,
    ret_sem,
    mixv,
    wx,
    wy,
    gaw,
    gxw,
    shiftv,
    xb,
    yb,
    av,
    bv,
    ends,
    halo_sem,
    ends_sem,
):
    n_ep = lax.axis_size("ep")
    nz = n_ep // 2
    ep = lax.axis_index("ep")
    t = lax.axis_index("tp")
    z, c = ep // 2, ep % 2
    y, x = t // 2, t % 2
    xp, yp, dg = y * 2 + (1 - x), (1 - y) * 2 + x, 3 - t
    pa, pb = jnp.where(c == 0, xp, yp), jnp.where(c == 0, yp, xp)
    other = z * 2 + (1 - c)
    rows, share = tok.shape[2], tok.shape[3]
    inner = (z > 0) & (z + 1 < nz)

    def block_at(s):
        q = jnp.int32(0)
        for zz in range(nz):
            q = jnp.where(z == zz, block_order[zz][s], q)
        return q

    def remote(src, dst, send, recv, where):
        return pltpu.make_async_remote_copy(
            src_ref=src,
            dst_ref=dst,
            send_sem=send,
            recv_sem=recv,
            device_id=where,
            device_id_type=MESH,
        )

    span = w2.shape[2]
    half = w2.shape[1] // 2

    def down_rows(k):
        return down_hbm.at[0, pl.ds(pl.multiple_of(k * half, half), half)]

    loads = [
        pltpu.make_async_copy(moe_hbm, nrm, load_sem.at[0]),
        pltpu.make_async_copy(gate_hbm.at[0], gw, load_sem.at[1]),
        pltpu.make_async_copy(up_hbm.at[0], uw, load_sem.at[2]),
        pltpu.make_async_copy(mix_hbm, mixv, load_sem.at[3]),
        pltpu.make_async_copy(wx_hbm, wx, load_sem.at[4]),
        pltpu.make_async_copy(wy_hbm, wy, load_sem.at[5]),
        pltpu.make_async_copy(ga_hbm, gaw, load_sem.at[6]),
        pltpu.make_async_copy(gx_hbm, gxw, load_sem.at[7]),
        pltpu.make_async_copy(shift_hbm, shiftv, load_sem.at[8]),
        pltpu.make_async_copy(down_rows(t), w2.at[0, pl.ds(0, half)], load_sem.at[9]),
        pltpu.make_async_copy(down_rows(pa), w2.at[0, pl.ds(half, half)], load_sem.at[10]),
    ]
    loads[0].start()
    barrier = pltpu.get_barrier_semaphore()
    for by in range(1, n_ep):
        pl.semaphore_signal(
            barrier, inc=1, device_id={"ep": (ep + by) % n_ep}, device_id_type=MESH
        )
    for peer in (xp, yp):
        for near in (ep, other):
            pl.semaphore_signal(
                barrier, inc=1, device_id={"ep": near, "tp": peer}, device_id_type=MESH
            )
    for copy in loads[3:6] + loads[1:3] + loads[6:]:
        copy.start()

    def columns(k):
        return pl.ds(pl.multiple_of(k * share, share), share)

    def z_own(k, up):
        return remote(
            nrm.at[:, columns((t, dg)[k])],
            tok.at[z, k],
            z_send.at[up, k, z],
            z_recv.at[k, z],
            {"ep": ep + (2 if up else -2)},
        )

    def z_copy(q, k, up):
        return remote(
            tok.at[q, k],
            tok.at[q, k],
            z_send.at[up, k, q],
            z_recv.at[k, q],
            {"ep": ep + (2 if up else -2)},
        )

    def route_copy(q):
        return remote(rt_row, routes_all.at[z], rt_sem.at[0, q], rt_sem.at[1, z], {"ep": q * 2 + c})

    def w_copy(k):
        piece = half // 2
        first = (pb, dg)[k // 2] * half + k % 2 * piece
        return remote(
            down_hbm.at[0, pl.ds(pl.multiple_of(first, piece), piece)],
            w2.at[1, pl.ds(k * piece, piece)],
            w_sem.at[0, k],
            w_sem.at[1, k],
            {"tp": pb},
        )

    def xs_part(q, block, k):
        return xs.at[q, pl.ds(pl.multiple_of(block * cap, cap), cap), columns(k)]

    def x_copy(q, kind):
        to = (xp, yp, xp, yp, t, t)[kind]
        near = ep if kind < 2 else other
        src = xs_part(q, c, t) if kind < 2 else stage.at[q, kind // 5]
        return remote(
            src,
            xs_part(q, c, dg if kind == 5 else t),
            x_send.at[kind, q],
            x_recv.at[kind, q],
            {"ep": near, "tp": to},
        )

    def x_wait(q, kind):
        block = c if kind < 2 else 1 - c
        dst = xs_part(q, block, (xp, yp, xp, yp, t, dg)[kind])
        remote(
            stage.at[q, 0], dst, x_send.at[kind, q], x_recv.at[kind, q], {"ep": other}
        ).wait_recv()

    def own_copy(block):
        return remote(
            own_stage,
            xs.at[z, pl.ds(pl.multiple_of(block * cap, cap), cap)],
            x_send.at[4, z],
            x_recv.at[4, z],
            {"ep": other},
        )

    def ag_copy(q, cc):
        at, sem = pl.ds(cc * cap, cap), q * 2 + cc
        return remote(
            hid.at[q, at, pl.ds(0, half)],
            hid.at[q, at, pl.ds(half, half)],
            ag_sem.at[0, sem],
            ag_sem.at[1, sem],
            {"tp": pa},
        )

    def rs_copy(q, cc):
        at, sem = pl.ds(cc * cap, cap), q * 2 + cc
        return remote(
            psend.at[q, at], precv.at[q, at], rs_sem.at[0, sem], rs_sem.at[1, sem], {"tp": pb}
        )

    def ret_copy(q, cc):
        return remote(
            res.at[q, pl.ds(cc * cap, cap)],
            ret.at[ep],
            ret_sem.at[0, q * 2 + cc],
            ret_sem.at[1, ep],
            {"ep": q * 2 + cc},
        )

    def arrive(q, k):
        z_copy(q, k, 1).wait_recv()

        @pl.when((q < z) & (z + 1 < nz))
        def _():
            z_copy(q, k, 1).start()

        @pl.when((q > z) & (z > 0))
        def _():
            z_copy(q, k, 0).start()

    def make_picks(q, named):
        lane = lax.broadcasted_iota(jnp.int32, (8, rows), 0)
        which = z * 2 + jnp.where(lane == 0, c, 1 - c)
        mask = jnp.where((named[0:1] == which) | (named[1:2] == which), 1.0, 0.0)
        before = jnp.where(
            lax.broadcasted_iota(jnp.int32, (rows, rows), 0)
            < lax.broadcasted_iota(jnp.int32, (rows, rows), 1),
            1.0,
            0.0,
        ).astype(BF16)
        rank = jnp.dot(mask.astype(BF16), before, preferred_element_type=F32)
        key = jnp.where(mask > 0.5, rank, -1.0)
        seat = lax.broadcasted_iota(jnp.int32, (cap, rows), 0).astype(F32)
        for k in range(2):
            picks[q, k * cap : (k + 1) * cap] = jnp.where(
                seat == key[k : k + 1], 1.0, 0.0
            ).astype(BF16)

    def pick_own():
        for k in range(4):
            at = pl.ds(k * share, share)
            got = jnp.dot(picks[z], nrm[:, at], preferred_element_type=F32).astype(BF16)
            xs[z, pl.ds(pl.multiple_of(c * cap, cap), cap), at] = got[:cap]
            own_stage[:, at] = got[cap:]
        own_copy(c).start()

    def pick(q, k):
        got = jnp.dot(picks[q], tok[q, k], preferred_element_type=F32).astype(BF16)
        xs[q, pl.ds(pl.multiple_of(c * cap, cap), cap), columns((t, dg)[k])] = got[:cap]
        stage[q, k] = got[cap:]
        for kind in (range(5), (5,))[k]:
            x_copy(q, kind).start()

    def gate_up(q):
        tile = 256

        @pl.loop(0, gw.shape[1] // tile)
        def _(j):
            cols = pl.ds(pl.multiple_of(j * tile, tile), tile)
            g = jnp.dot(xs[q], gw[:, cols], preferred_element_type=F32)
            u = jnp.dot(xs[q], uw[:, cols], preferred_element_type=F32)
            hid[q, :, cols] = (jax.nn.silu(g) * u).astype(BF16)

    def gathered(q):
        for kind in range(6):
            x_wait(q, kind)

    def ag_start(q):
        for cc in range(2):
            ag_copy(q, cc).start()

    def down(q):
        tile = 256
        for cc in range(2):
            at = pl.ds(cc * cap, cap)
            ag_copy(q, cc).wait_recv()

            @pl.loop(0, span // tile)
            def _(j):
                cols = pl.ds(pl.multiple_of(j * tile, tile), tile)
                psend[q, at, cols] = jnp.dot(
                    hid[q, at], w2[1, :, cols], preferred_element_type=F32
                ).astype(BF16)

            rs_copy(q, cc).start()

        @pl.loop(0, span // tile)
        def _(j):
            cols = pl.ds(pl.multiple_of(j * tile, tile), tile)
            pown[q, :, cols] = jnp.dot(hid[q], w2[0, :, cols], preferred_element_type=F32)

    def give(q):
        for cc in range(2):
            at = pl.ds(cc * cap, cap)
            rs_copy(q, cc).wait_recv()
            res[q, at] = (pown[q, at] + precv[q, at].astype(F32)).astype(BF16)
            ret_copy(q, cc).start()

    def give_own():
        for cc in range(2):
            at = pl.ds(cc * cap, cap)
            rs_copy(z, cc).wait_recv()
            res[z, at] = (pown[z, at] + precv[z, at].astype(F32)).astype(BF16)

            @pl.when(c != cc)
            def _():
                ret_copy(z, cc).start()

    pad = xb.shape[0] - rows

    def halo_copy():
        return remote(
            xb.at[pl.ds(rows, pad)],
            xb.at[pl.ds(0, pad)],
            halo_sem.at[0],
            halo_sem.at[1],
            {"ep": ep + 1},
        )

    def ends_copy(by):
        return remote(
            ends.at[ep],
            ends.at[ep],
            ends_sem.at[0, by],
            ends_sem.at[1, ep],
            {"ep": (ep + by) % n_ep},
        )

    def norm(buffer, gain):
        strip = 64

        @pl.loop(0, rows // strip)
        def _(i):
            at = pl.ds(pl.multiple_of(i * strip, strip), strip)
            wide = buffer[at, :].astype(F32)
            scale = lax.rsqrt(jnp.mean(wide * wide, axis=-1, keepdims=True) + epsilon)
            buffer[at, :] = (wide * scale * gain[...]).astype(BF16)

    def project():
        for k in range(3, 6):
            loads[k].wait()
        norm(mixv, mix_gain_ref)
        tile = 256

        @pl.loop(0, wx.shape[1] // tile)
        def _(j):
            cols = pl.ds(pl.multiple_of(j * tile, tile), tile)
            xb[pl.ds(pad, rows), cols] = jnp.dot(
                mixv[...], wx[:, cols], preferred_element_type=F32
            ).astype(BF16)
            yb[:, cols] = jnp.dot(mixv[...], wy[:, cols], preferred_element_type=F32).astype(BF16)

        @pl.when(ep + 1 < n_ep)
        def _():
            halo_copy().start()

        @pl.when(ep == 0)
        def _():
            xb[pl.ds(0, pad), :] = jnp.zeros((pad, xb.shape[1]), BF16)

    def drives_ready():
        for k in range(6, 9):
            loads[k].wait()

        @pl.when(ep > 0)
        def _():
            halo_copy().wait_recv()

    def drives(heads):
        taps = taps_ref.shape[0]
        size = gaw.shape[1]
        for h in heads:
            cols = pl.ds(h * size, size)
            wide = xb[:, cols].astype(F32)
            conv = jnp.zeros((rows, size), F32)
            for k in range(taps):
                first_row = pad - (taps - 1) + k
                conv = conv + taps_ref[k : k + 1, cols] * wide[first_row : first_row + rows]
            x_conv = conv.astype(BF16)
            gate_a = jnp.dot(x_conv, gaw[h], preferred_element_type=F32)
            gate_x = jnp.dot(x_conv, gxw[h], preferred_element_type=F32)
            log_decay = (
                -lru_scale * jax.nn.sigmoid(gate_a) * soft_plus(-logit_ref[:, cols])
                + shiftv[:, cols]
            )
            av[:, cols] = jnp.exp(log_decay)
            bv[:, cols] = (
                jnp.sqrt(one_minus_exp(2.0 * log_decay))
                * jax.nn.sigmoid(gate_x)
                * x_conv.astype(F32)
            )

    def recur():
        width = av.shape[1]
        row = lax.broadcasted_iota(jnp.int32, (8, width), 0)

        def group(i, carry):
            at = pl.ds(pl.multiple_of(i * 8, 8), 8)
            a, b = av[at, :], bv[at, :]
            for by in (1, 2, 4):
                a_past, b_past = pltpu.roll(a, by, 0), pltpu.roll(b, by, 0)
                b = jnp.where(row >= by, a * b_past + b, b)
                a = jnp.where(row >= by, a * a_past, a)
            b = a * carry[1] + b
            a = a * carry[0]
            av[at, :] = a
            bv[at, :] = b
            return (a[7:8], b[7:8])

        through, state = lax.fori_loop(
            0, rows // 8, group, (jnp.ones((1, width), F32), jnp.zeros((1, width), F32))
        )
        ends[ep, 0:1] = through
        ends[ep, 1:2] = state
        for by in range(1, n_ep):
            ends_copy(by).start()

    def finish():
        carried = jnp.zeros((1, av.shape[1]), F32)
        for by in range(1, n_ep):
            peer = (ep + by) % n_ep
            remote(
                ends.at[peer], ends.at[peer], ends_sem.at[0, 0], ends_sem.at[1, peer], {"ep": peer}
            ).wait_recv()
        for k in range(n_ep):
            entered = ends[k, 0:1] * carried + ends[k, 1:2]
            carried = jnp.where(k < ep, entered, carried)
        strip = 32

        @pl.loop(0, rows // strip)
        def _(i):
            at = pl.ds(pl.multiple_of(i * strip, strip), strip)
            state = bv[at, :] + av[at, :] * carried
            mix_ref[at, :] = (state * jax.nn.gelu(yb[at, :].astype(F32))).astype(BF16)

    def make_combine():
        weights = rw_row[...]
        sides = jnp.concatenate(
            [
                rt_row[...].astype(F32),
                weights / (weights[0:1] + weights[1:2]),
                jnp.zeros((124, rows), F32),
            ],
            axis=0,
        ).T
        one, two = sides[:, 0:1].astype(jnp.int32), sides[:, 1:2].astype(jnp.int32)
        lane = lax.broadcasted_iota(jnp.int32, (rows, 128), 1)
        mask = jnp.where((one == lane) | (two == lane), 1.0, 0.0)
        before = jnp.where(
            lax.broadcasted_iota(jnp.int32, (rows, rows), 1)
            < lax.broadcasted_iota(jnp.int32, (rows, rows), 0),
            1.0,
            0.0,
        ).astype(BF16)
        rank = jnp.dot(before, mask.astype(BF16), preferred_element_type=F32)
        key = jnp.where(mask > 0.5, rank, -1.0)
        part_one, part_two = sides[:, 2:3], sides[:, 3:4]
        seat = lax.broadcasted_iota(jnp.int32, (rows, cap), 1).astype(F32)
        for e in range(n_ep):
            comb[e] = jnp.where(seat == key[:, e : e + 1], 1.0, 0.0).astype(BF16)
            part[e] = jnp.broadcast_to(
                jnp.where(one == e, part_one, 0.0) + jnp.where(two == e, part_two, 0.0),
                (rows, 128),
            )

    def combine(e, rows_in, first=False, last=False):
        got = jnp.dot(comb[e], rows_in, preferred_element_type=F32)
        for j in range(got.shape[1] // 128):
            at = pl.ds(j * 128, 128)
            term = part[e] * got[:, j * 128 : (j + 1) * 128]
            if not first:
                term = total[:, at] + term
            if last:
                out_ref[:, at] = term.astype(BF16)
            else:
                total[:, at] = term

    def ret_wait(e):
        remote(
            res.at[0, pl.ds(0, cap)], ret.at[e], ret_sem.at[0, 0], ret_sem.at[1, e], {"ep": other}
        ).wait_recv()

    def combine_plane(q, first=False, last=False):
        for cc in range(2):
            ret_wait(q * 2 + cc)
            combine(q * 2 + cc, ret[q * 2 + cc], first and cc == 0, last and cc == 1)

    loads[0].wait()
    norm(nrm, gain_ref)
    pl.semaphore_wait(barrier, n_ep + 3)
    for q in range(nz):

        @pl.when(q != z)
        def _():
            route_copy(q).start()

    for k in range(2):

        @pl.when(z + 1 < nz)
        def _():
            z_own(k, 1).start()

        @pl.when(z > 0)
        def _():
            z_own(k, 0).start()

    for k in range(3):
        w_copy(k).start()
    make_picks(z, rt_row[...])
    pick_own()
    project()
    one, two, three = block_at(0), block_at(1), block_at(2)
    for q in (one, two, three):
        remote(
            rt_row, routes_all.at[q], rt_sem.at[0, 0], rt_sem.at[1, q], {"ep": q * 2 + c}
        ).wait_recv()
        make_picks(q, routes_all[q])
    own_copy(1 - c).wait_recv()
    for k in range(1, 3):
        loads[k].wait()
    gate_up(z)
    arrive(one, 0)
    pick(one, 0)
    w_copy(3).start()

    @pl.when(inner)
    def _():
        arrive(three, 0)

    drives_ready()
    drives(range(0, 4))
    make_combine()
    arrive(one, 1)
    pick(one, 1)

    @pl.when(inner)
    def _():
        arrive(three, 1)

    recur()
    gathered(one)
    gate_up(one)
    ag_start(one)
    arrive(two, 0)
    pick(two, 0)
    for k in range(9, 11):
        loads[k].wait()
    for k in range(4):
        w_copy(k).wait_recv()
    down(one)
    arrive(two, 1)
    pick(two, 1)
    gathered(two)
    gate_up(two)
    ag_start(two)
    give(one)

    @pl.when(jnp.logical_not(inner))
    def _():
        arrive(three, 0)

    pick(three, 0)
    down(two)
    finish()

    @pl.when(jnp.logical_not(inner))
    def _():
        arrive(three, 1)

    pick(three, 1)
    give(two)
    gathered(three)
    gate_up(three)
    ag_start(three)
    combine_plane(one, first=True)
    down(three)
    ag_start(z)
    give(three)
    down(z)
    combine_plane(two)
    give_own()
    combine(ep, res[z, pl.ds(pl.multiple_of(c * cap, cap), cap)])
    ret_wait(other)
    combine(other, ret[other])
    combine_plane(three, last=True)

    for k in range(2):

        @pl.when(z + 1 < nz)
        def _():
            z_own(k, 1).wait_send()

        @pl.when(z > 0)
        def _():
            z_own(k, 0).wait_send()

    for k in range(4):
        w_copy(k).wait_send()

    own_copy(c).wait_send()

    @pl.when(ep + 1 < n_ep)
    def _():
        halo_copy().wait_send()

    for by in range(1, n_ep):
        ends_copy(by).wait_send()

    def drain(q, carry):
        for cc in range(2):
            ag_copy(q, cc).wait_send()
            rs_copy(q, cc).wait_send()

        @pl.when(q != z)
        def _():
            route_copy(q).wait_send()
            for kind in range(6):
                x_copy(q, kind).wait_send()

        for k in range(2):

            @pl.when((q < z) & (z + 1 < nz))
            def _():
                z_copy(q, k, 1).wait_send()

            @pl.when((q > z) & (z > 0))
            def _():
                z_copy(q, k, 0).wait_send()

        for cc in range(2):

            @pl.when((q != z) | (c != cc))
            def _():
                ret_copy(q, cc).wait_send()

        return carry

    lax.fori_loop(0, nz, drain, 0)


def both_fused(
    mix_in,
    mix_gain,
    w_in_x,
    w_in_y,
    conv_taps,
    recur_gate_w,
    input_gate_w,
    decay_logit,
    decay_shift,
    moe_in,
    moe_gain,
    routes,
    route_weight,
    expert_gate,
    expert_up,
    expert_down,
):
    n_ep = lax.axis_size("ep")
    nz = n_ep // 2
    rows, features = moe_in.shape
    share = features // 4
    ff_dev, out_dev = expert_gate.shape[2], expert_down.shape[2]
    width = w_in_x.shape[1]
    cap = 2 * rows * routes.shape[1] // n_ep
    pair = 2 * cap
    vmem = pl.BlockSpec(memory_space=pltpu.VMEM)
    hbm = pl.BlockSpec(memory_space=pltpu.HBM)
    dma = pltpu.SemaphoreType.DMA
    flops = 2 * n_ep * cap * features * (2 * ff_dev + out_dev)
    return pl.pallas_call(
        functools.partial(both_kernel, cap),
        out_shape=(
            jax.ShapeDtypeStruct((rows, width), BF16),
            jax.ShapeDtypeStruct((rows, out_dev), BF16),
        ),
        in_specs=[hbm] * 6 + [vmem] * 3 + [hbm] + [vmem] * 3 + [hbm] * 3,
        out_specs=(vmem, vmem),
        scratch_shapes=[
            pltpu.VMEM((rows, features), BF16),
            pltpu.VMEM((nz, 2, rows, share), BF16),
            pltpu.VMEM((nz, pair, features), BF16),
            pltpu.VMEM((nz, 2, cap, share), BF16),
            pltpu.VMEM((cap, features), BF16),
            pltpu.VMEM((nz, pair, rows), BF16),
            pltpu.VMEM((nz, pair, 2 * ff_dev), BF16),
            pltpu.VMEM((nz, pair, out_dev), BF16),
            pltpu.VMEM((nz, pair, out_dev), BF16),
            pltpu.VMEM((nz, pair, out_dev), F32),
            pltpu.VMEM((nz, pair, out_dev), BF16),
            pltpu.VMEM((n_ep, cap, out_dev), BF16),
            pltpu.VMEM((nz, 2, rows), jnp.int32),
            pltpu.VMEM((n_ep, rows, cap), BF16),
            pltpu.VMEM((n_ep, rows, 128), F32),
            pltpu.VMEM((rows, out_dev), F32),
            pltpu.VMEM(expert_gate.shape[1:], BF16),
            pltpu.VMEM(expert_up.shape[1:], BF16),
            pltpu.VMEM((2, 2 * ff_dev, out_dev), BF16),
            dma((11,)),
            dma((2, nz)),
            dma((2, 2, nz)),
            dma((2, nz)),
            dma((2, 4)),
            dma((6, nz)),
            dma((6, nz)),
            dma((2, n_ep)),
            dma((2, n_ep)),
            dma((2, n_ep)),
            pltpu.VMEM(mix_in.shape, BF16),
            pltpu.VMEM(w_in_x.shape, BF16),
            pltpu.VMEM(w_in_y.shape, BF16),
            pltpu.VMEM(recur_gate_w.shape, BF16),
            pltpu.VMEM(input_gate_w.shape, BF16),
            pltpu.VMEM((rows, width), F32),
            pltpu.VMEM((16 + rows, width), BF16),
            pltpu.VMEM((rows, width), BF16),
            pltpu.VMEM((rows, width), F32),
            pltpu.VMEM((rows, width), F32),
            pltpu.VMEM((n_ep, 2, width), F32),
            dma((2,)),
            dma((2, n_ep)),
        ],
        compiler_params=pltpu.CompilerParams(
            collective_id=0, has_side_effects=True, vmem_limit_bytes=60 * 1024 * 1024
        ),
        cost_estimate=pl.CostEstimate(flops=flops, bytes_accessed=16 << 20, transcendentals=0),
        name="both",
    )(
        mix_in,
        w_in_x,
        w_in_y,
        recur_gate_w,
        input_gate_w,
        decay_shift,
        mix_gain[None, :],
        conv_taps,
        decay_logit[None, :],
        moe_in,
        moe_gain[None, :],
        routes.T,
        route_weight.T,
        expert_gate,
        expert_up,
        expert_down,
    )


def from_behind(value, axis, by):
    count = lax.axis_size(axis)
    pairs = [(i, i + by) for i in range(count) if 0 <= i + by < count]
    return lax.ppermute(value, axis, pairs)


def entering(value, axis, combine, identity):
    count, index = (lax.axis_size(axis), lax.axis_index(axis))
    everything = jax.tree.map(lambda part: lax.all_gather(part, axis), value)
    start = jax.tree.map(
        lambda part, zero: jnp.broadcast_to(jnp.asarray(zero, part.dtype), part.shape),
        value,
        identity,
    )

    def hop(k, before):
        reached = k < index
        new = combine(before, jax.tree.map(lambda part: part[k], everything))
        return jax.tree.map(lambda a, b: jnp.where(reached, a, b), new, before)

    return lax.fori_loop(0, count, hop, start)


def norm_rows(rows, gain):
    widened = rows.astype(jnp.float32)
    scaled = widened * lax.rsqrt(jnp.mean(widened * widened, axis=-1, keepdims=True) + epsilon)
    return (scaled * gain[None, :]).astype(jnp.bfloat16)


def link(earlier, later):
    return (earlier[0] * later[0], later[0] * earlier[1] + later[1])


def fits_fused(moe_in, routes):
    n_ep = lax.axis_size("ep")
    gathered = n_ep * moe_in.size * moe_in.dtype.itemsize
    even = n_ep == 4 * routes.shape[1] == 2 * len(block_order)
    return lax.axis_size("tp") == 4 and even and gathered <= (16 << 20)


def moe_staged(moe_in, moe_gain, routes, route_weight, expert_gate, expert_up, expert_down):
    moe_rows = norm_rows(moe_in, moe_gain)
    token_count = moe_rows.shape[0]
    feature_count = moe_rows.shape[1]
    choose_count = routes.shape[1]
    expert_count = lax.axis_size("ep")
    capacity = 2 * token_count * choose_count // expert_count
    slot_total = expert_count * capacity
    expert_ids = routes.reshape(-1)
    onehot = (expert_ids[:, None] == jnp.arange(expert_count, dtype=jnp.int32)[None, :]).astype(
        jnp.int32
    )
    slot_rank = jnp.sum(jnp.cumsum(onehot, axis=0) * onehot, axis=1) - 1
    slot_index = expert_ids * capacity + slot_rank
    token_index = jnp.repeat(jnp.arange(token_count, dtype=jnp.int32), choose_count)
    slot_owner = jnp.full((slot_total,), token_count, jnp.int32).at[slot_index].set(token_index)
    padded_rows = jnp.concatenate([moe_rows, jnp.zeros((1, feature_count), jnp.bfloat16)], axis=0)
    outgoing = padded_rows[slot_owner].reshape(expert_count, capacity, feature_count)
    column_width = feature_count // lax.axis_size("tp")
    own_columns = lax.dynamic_slice_in_dim(
        outgoing, lax.axis_index("tp") * column_width, column_width, 2
    )
    incoming = lax.all_to_all(own_columns, "ep", split_axis=0, concat_axis=0, tiled=True)
    piece = lax.all_gather(incoming, "tp", axis=2, tiled=True)
    flat_rows = piece.reshape(slot_total, piece.shape[2])
    gate_rows = expert_gate[0]
    up_rows = expert_up[0]
    gate_proj = jnp.dot(flat_rows, gate_rows, preferred_element_type=jnp.float32)
    up_proj = jnp.dot(flat_rows, up_rows, preferred_element_type=jnp.float32)
    hidden = (jax.nn.silu(gate_proj) * up_proj).astype(jnp.bfloat16)
    down_rows = expert_down[0]
    columns = jnp.dot(
        lax.all_gather(hidden, "tp", axis=1, tiled=True),
        down_rows,
        preferred_element_type=jnp.float32,
    )
    results = columns.astype(jnp.bfloat16).reshape(expert_count, capacity, expert_down.shape[2])
    returned = lax.all_to_all(results, "ep", split_axis=0, concat_axis=0, tiled=True).reshape(
        slot_total, expert_down.shape[2]
    )
    picked = (
        returned[slot_index]
        .astype(jnp.float32)
        .reshape(token_count, choose_count, expert_down.shape[2])
    )
    route_share = route_weight / jnp.sum(route_weight, axis=1, keepdims=True)
    moe_out = jnp.sum(route_share[:, :, None] * picked, axis=1).astype(jnp.bfloat16)
    return moe_out


def staged(
    mix_in,
    mix_gain,
    w_in_x,
    w_in_y,
    conv_taps,
    recur_gate_w,
    input_gate_w,
    decay_logit,
    decay_shift,
    moe_in,
    moe_gain,
    routes,
    route_weight,
    expert_gate,
    expert_up,
    expert_down,
):
    row_count = mix_in.shape[0]
    width_dev = w_in_x.shape[1]
    heads_dev = recur_gate_w.shape[0]
    block_size = recur_gate_w.shape[1]
    tap_count = conv_taps.shape[0]
    mixer_rows = norm_rows(mix_in, mix_gain)
    x_branch = jnp.dot(mixer_rows, w_in_x, preferred_element_type=jnp.float32).astype(jnp.bfloat16)
    y_branch = jnp.dot(mixer_rows, w_in_y, preferred_element_type=jnp.float32).astype(jnp.bfloat16)
    previous = from_behind(x_branch[row_count - (tap_count - 1) :], "ep", 1)
    padded = jnp.concatenate([previous, x_branch], axis=0)
    conv_sum = jnp.zeros((row_count, width_dev), jnp.float32)
    for tap_index in range(tap_count):
        conv_sum = conv_sum + conv_taps[tap_index][None, :] * padded[
            tap_index : tap_index + row_count
        ].astype(jnp.float32)
    x_conv = conv_sum.astype(jnp.bfloat16)
    heads_in = x_conv.reshape(row_count, heads_dev, block_size)
    gate_a = jnp.einsum(
        "thi,hij->thj", heads_in, recur_gate_w, preferred_element_type=jnp.float32
    ).reshape(row_count, width_dev)
    gate_x = jnp.einsum(
        "thi,hij->thj", heads_in, input_gate_w, preferred_element_type=jnp.float32
    ).reshape(row_count, width_dev)
    log_decay = (
        -lru_scale * jax.nn.sigmoid(gate_a) * jax.nn.softplus(-decay_logit)[None, :] + decay_shift
    )
    lru_drive = (
        jnp.sqrt(-jnp.expm1(2.0 * log_decay)) * jax.nn.sigmoid(gate_x) * x_conv.astype(jnp.float32)
    )
    through, local_state = lax.associative_scan(link, (jnp.exp(log_decay), lru_drive), axis=0)
    identity = (jnp.ones((width_dev,), jnp.float32), jnp.zeros((width_dev,), jnp.float32))
    carried = entering((through[row_count - 1], local_state[row_count - 1]), "ep", link, identity)
    lru_state = local_state + through * carried[1][None, :]
    mixer_out = (lru_state * jax.nn.gelu(y_branch.astype(jnp.float32))).astype(jnp.bfloat16)
    moe_out = moe_staged(
        moe_in, moe_gain, routes, route_weight, expert_gate, expert_up, expert_down
    )
    return (mixer_out, moe_out)


def local(*args):
    return (both_fused if fits_fused(args[9], args[11]) else staged)(*args)


def solution(mesh):
    placed = (
        P("ep", None),
        P(),
        P(None, "tp"),
        P(None, "tp"),
        P(None, "tp"),
        P("tp", None, None),
        P("tp", None, None),
        P("tp"),
        P("ep", "tp"),
        P("ep", None),
        P(),
        P("ep", None),
        P("ep", None),
        P("ep", None, "tp"),
        P("ep", None, "tp"),
        P("ep", None, "tp"),
    )
    return jax.shard_map(
        local, mesh=mesh, in_specs=placed, out_specs=(P("ep", "tp"), P("ep", "tp")), check_vma=False
    )
```

time: 94.5 us -> 80.1 us (0.85)
  Pallas kernels: 89 us -> 75.9 us
  other arithmetic: 1.28 us -> 0 us
    pallas_call x1, Pallas kernels: 89 us -> 75.9 us  [both_fused(): pl.pallas_call(functools.partial(both_kernel, cap), out_shape=(jax.ShapeD...]
    select_n x1 -> x0, other arithmetic: 1.28 us -> none  [both_fused(): jax.nn.softplus(-decay_logit)[None, :]]
where the time goes in v1:
time: 80.1 us; the launch traced here: 79.9 us
  Pallas kernels  75.9 us (95%)
  local copies, waits for them, and re-layouts  3.34 us (4%)
    pallas_call x1, Pallas kernels, both_fused(): pl.pallas_call(functools.partial(both_kernel, cap), out_shape=(jax.ShapeD...  75.9 us
    unnamed x2, local copies, waits for them, and re-layouts  3.34 us

profile of v1, /device:TPU:1, one launch (start us, length us, event | category | flops | bytes accessed | tf_op | source)
XLA Modules:
  0.0 79.9 jit_solution(12311244360708823867)
XLA Ops:
  0.6 75.9 %both.1 = (bf16[256,512]{1,0:T(8,128)(2,1)}, bf16[256,512]{1,0:T(8,128)(2,1)}) custom-call(bf16[256,2048]{1,0:T(8,128)(2,1)} %mix_hbm.1, bf16[2048,512]{1,0:T(8,128)(2,1)} %wx_hbm.1, bf16[2048,512]{1,0:T(8,128)(2,1)} %wy_hbm.1, bf16[4,128,128]{2,1,0:T(8,128)(2,1)} %ga_hbm.1, bf16[4,128,128]{2,1,0:T(8,128)(2,1)} %gx_hbm.1, f32[256,512]{1,0:T(8,128)} %shift_hbm.1, ...), custom_call_target="tpu_custom_call" | custom-call | flops 6442450944 | bytes 16777216 | tf_op jit(solution)/shard_map/both/pallas_call | solution.py:713
  76.5 1.7 %copy.20 = bf16[256,512]{1,0:T(8,128)(2,1)} copy(bf16[256,512]{1,0:T(8,128)(2,1)} %get-tuple-element.4) | data formatting | bytes 524288
  78.2 1.7 %copy.21 = bf16[256,512]{1,0:T(8,128)(2,1)} copy(bf16[256,512]{1,0:T(8,128)(2,1)} %get-tuple-element.5) | data formatting | bytes 524288

commit v2 on v1

--- a/solution.py
+++ b/solution.py
@@ -14,7 +14,7 @@
 BF16 = jnp.bfloat16
 
 
-block_order = ((1, 2, 3), (0, 3, 2), (3, 0, 1), (2, 1, 0))
+block_order = ((1, 2, 3), (2, 3, 0), (1, 0, 3), (2, 1, 0))
 
 
 def one_minus_exp(value):
@@ -108,6 +108,8 @@
     other = z * 2 + (1 - c)
     rows, share = tok.shape[2], tok.shape[3]
     inner = (z > 0) & (z + 1 < nz)
+    outer = jnp.logical_not(inner)
+    shares = (t, dg, xp, yp)
 
     def block_at(s):
         q = jnp.int32(0)
@@ -163,7 +165,7 @@
 
     def z_own(k, up):
         return remote(
-            nrm.at[:, columns((t, dg)[k])],
+            nrm.at[:, columns(shares[k])],
             tok.at[z, k],
             z_send.at[up, k, z],
             z_recv.at[k, z],
@@ -197,12 +199,12 @@
         return xs.at[q, pl.ds(pl.multiple_of(block * cap, cap), cap), columns(k)]
 
     def x_copy(q, kind):
-        to = (xp, yp, xp, yp, t, t)[kind]
+        to = (xp, yp, xp, yp, t, t, t, t)[kind]
         near = ep if kind < 2 else other
-        src = xs_part(q, c, t) if kind < 2 else stage.at[q, kind // 5]
+        src = xs_part(q, c, t) if kind < 2 else stage.at[q, max(kind - 4, 0)]
         return remote(
             src,
-            xs_part(q, c, dg if kind == 5 else t),
+            xs_part(q, c, shares[max(kind - 4, 0)]),
             x_send.at[kind, q],
             x_recv.at[kind, q],
             {"ep": near, "tp": to},
@@ -210,7 +212,7 @@
 
     def x_wait(q, kind):
         block = c if kind < 2 else 1 - c
-        dst = xs_part(q, block, (xp, yp, xp, yp, t, dg)[kind])
+        dst = xs_part(q, block, (xp, yp, xp, yp, t, dg, xp, yp)[kind])
         remote(
             stage.at[q, 0], dst, x_send.at[kind, q], x_recv.at[kind, q], {"ep": other}
         ).wait_recv()
@@ -251,14 +253,15 @@
 
     def arrive(q, k):
         z_copy(q, k, 1).wait_recv()
-
-        @pl.when((q < z) & (z + 1 < nz))
-        def _():
-            z_copy(q, k, 1).start()
-
-        @pl.when((q > z) & (z > 0))
-        def _():
-            z_copy(q, k, 0).start()
+        if k < 2:
+
+            @pl.when((q < z) & (z + 1 < nz))
+            def _():
+                z_copy(q, k, 1).start()
+
+            @pl.when((q > z) & (z > 0))
+            def _():
+                z_copy(q, k, 0).start()
 
     def make_picks(q, named):
         lane = lax.broadcasted_iota(jnp.int32, (8, rows), 0)
@@ -286,11 +289,11 @@
             own_stage[:, at] = got[cap:]
         own_copy(c).start()
 
-    def pick(q, k):
+    def pick(q, k, whole=False):
         got = jnp.dot(picks[q], tok[q, k], preferred_element_type=F32).astype(BF16)
-        xs[q, pl.ds(pl.multiple_of(c * cap, cap), cap), columns((t, dg)[k])] = got[:cap]
+        xs[q, pl.ds(pl.multiple_of(c * cap, cap), cap), columns(shares[k])] = got[:cap]
         stage[q, k] = got[cap:]
-        for kind in (range(5), (5,))[k]:
+        for kind in range(5) if k == 0 and not whole else (4 + k,):
             x_copy(q, kind).start()
 
     def gate_up(q):
@@ -303,40 +306,41 @@
             u = jnp.dot(xs[q], uw[:, cols], preferred_element_type=F32)
             hid[q, :, cols] = (jax.nn.silu(g) * u).astype(BF16)
 
-    def gathered(q):
-        for kind in range(6):
+    def gathered(q, kinds=range(6)):
+        for kind in kinds:
             x_wait(q, kind)
 
     def ag_start(q):
         for cc in range(2):
             ag_copy(q, cc).start()
 
-    def down(q):
+    def down_other(q, cc):
         tile = 256
-        for cc in range(2):
-            at = pl.ds(cc * cap, cap)
-            ag_copy(q, cc).wait_recv()
-
-            @pl.loop(0, span // tile)
-            def _(j):
-                cols = pl.ds(pl.multiple_of(j * tile, tile), tile)
-                psend[q, at, cols] = jnp.dot(
-                    hid[q, at], w2[1, :, cols], preferred_element_type=F32
-                ).astype(BF16)
-
-            rs_copy(q, cc).start()
+        at = pl.ds(cc * cap, cap)
+        ag_copy(q, cc).wait_recv()
+
+        @pl.loop(0, span // tile)
+        def _(j):
+            cols = pl.ds(pl.multiple_of(j * tile, tile), tile)
+            psend[q, at, cols] = jnp.dot(
+                hid[q, at], w2[1, :, cols], preferred_element_type=F32
+            ).astype(BF16)
+
+        rs_copy(q, cc).start()
+
+    def down_own(q):
+        tile = 256
 
         @pl.loop(0, span // tile)
         def _(j):
             cols = pl.ds(pl.multiple_of(j * tile, tile), tile)
             pown[q, :, cols] = jnp.dot(hid[q], w2[0, :, cols], preferred_element_type=F32)
 
-    def give(q):
-        for cc in range(2):
-            at = pl.ds(cc * cap, cap)
-            rs_copy(q, cc).wait_recv()
-            res[q, at] = (pown[q, at] + precv[q, at].astype(F32)).astype(BF16)
-            ret_copy(q, cc).start()
+    def give(q, cc):
+        at = pl.ds(cc * cap, cap)
+        rs_copy(q, cc).wait_recv()
+        res[q, at] = (pown[q, at] + precv[q, at].astype(F32)).astype(BF16)
+        ret_copy(q, cc).start()
 
     def give_own():
         for cc in range(2):
@@ -522,10 +526,9 @@
             res.at[0, pl.ds(0, cap)], ret.at[e], ret_sem.at[0, 0], ret_sem.at[1, e], {"ep": other}
         ).wait_recv()
 
-    def combine_plane(q, first=False, last=False):
-        for cc in range(2):
-            ret_wait(q * 2 + cc)
-            combine(q * 2 + cc, ret[q * 2 + cc], first and cc == 0, last and cc == 1)
+    def combine_far(e, first=False, last=False):
+        ret_wait(e)
+        combine(e, ret[e], first, last)
 
     loads[0].wait()
     norm(nrm, gain_ref)
@@ -536,13 +539,13 @@
         def _():
             route_copy(q).start()
 
-    for k in range(2):
-
-        @pl.when(z + 1 < nz)
+    for k in range(4):
+
+        @pl.when((z + 1 < nz) & ((z == 0) | (k < 2)))
         def _():
             z_own(k, 1).start()
 
-        @pl.when(z > 0)
+        @pl.when((z > 0) & ((z + 1 == nz) | (k < 2)))
         def _():
             z_own(k, 0).start()
 
@@ -550,13 +553,13 @@
         w_copy(k).start()
     make_picks(z, rt_row[...])
     pick_own()
-    project()
     one, two, three = block_at(0), block_at(1), block_at(2)
     for q in (one, two, three):
         remote(
             rt_row, routes_all.at[q], rt_sem.at[0, 0], rt_sem.at[1, q], {"ep": q * 2 + c}
         ).wait_recv()
         make_picks(q, routes_all[q])
+    project()
     own_copy(1 - c).wait_recv()
     for k in range(1, 3):
         loads[k].wait()
@@ -569,8 +572,6 @@
     def _():
         arrive(three, 0)
 
-    drives_ready()
-    drives(range(0, 4))
     make_combine()
     arrive(one, 1)
     pick(one, 1)
@@ -579,7 +580,6 @@
     def _():
         arrive(three, 1)
 
-    recur()
     gathered(one)
     gate_up(one)
     ag_start(one)
@@ -589,50 +589,85 @@
         loads[k].wait()
     for k in range(4):
         w_copy(k).wait_recv()
-    down(one)
+    down_other(one, 0)
+    down_other(one, 1)
+    down_own(one)
     arrive(two, 1)
     pick(two, 1)
     gathered(two)
     gate_up(two)
     ag_start(two)
-    give(one)
-
-    @pl.when(jnp.logical_not(inner))
+    drives_ready()
+    drives(range(0, 4))
+    give(one, 0)
+    give(one, 1)
+    recur()
+
+    @pl.when(outer)
     def _():
         arrive(three, 0)
-
-    pick(three, 0)
-    down(two)
-    finish()
-
-    @pl.when(jnp.logical_not(inner))
+        pick(three, 0)
+
+    @pl.when(inner)
+    def _():
+        pick(three, 0, True)
+
+    down_other(two, 0)
+    ag_start(z)
+    down_other(two, 1)
+    down_own(two)
+
+    @pl.when(outer)
     def _():
         arrive(three, 1)
-
-    pick(three, 1)
-    give(two)
-    gathered(three)
+        pick(three, 1)
+
+    @pl.when(inner)
+    def _():
+        pick(three, 1)
+        for k in range(2, 4):
+            arrive(three, k)
+            pick(three, k)
+
+
+    @pl.when(outer)
+    def _():
+        gathered(three)
+
+    @pl.when(inner)
+    def _():
+        gathered(three, range(4, 8))
+
     gate_up(three)
     ag_start(three)
-    combine_plane(one, first=True)
-    down(three)
-    ag_start(z)
-    give(three)
-    down(z)
-    combine_plane(two)
+    give(two, 0)
+    give(two, 1)
+    finish()
+    down_other(three, 0)
+    down_other(three, 1)
+    down_own(three)
+    give(three, 0)
+    give(three, 1)
+    down_other(z, 0)
+    down_other(z, 1)
+    down_own(z)
+    combine_far(two * 2 + 0, first=True)
+    combine_far(two * 2 + 1)
+    combine_far(one * 2 + 0)
+    combine_far(one * 2 + 1)
     give_own()
     combine(ep, res[z, pl.ds(pl.multiple_of(c * cap, cap), cap)])
-    ret_wait(other)
-    combine(other, ret[other])
-    combine_plane(three, last=True)
-
-    for k in range(2):
-
-        @pl.when(z + 1 < nz)
+    combine_far(other)
+    combine_far(three * 2 + 0)
+    combine_far(three * 2 + 1, last=True)
+
+    for k in range(4):
+
+        @pl.when((z + 1 < nz) & ((z == 0) | (k < 2)))
         def _():
             z_own(k, 1).wait_send()
 
-        @pl.when(z > 0)
+        @pl.when((z > 0) & ((z + 1 == nz) | (k < 2)))
         def _():
             z_own(k, 0).wait_send()
 
@@ -656,7 +691,19 @@
         @pl.when(q != z)
         def _():
             route_copy(q).wait_send()
-            for kind in range(6):
+            for kind in range(4, 6):
+                x_copy(q, kind).wait_send()
+
+        whole = inner & (q == block_at(2))
+
+        @pl.when((q != z) & jnp.logical_not(whole))
+        def _():
+            for kind in range(4):
+                x_copy(q, kind).wait_send()
+
+        @pl.when(whole)
+        def _():
+            for kind in range(6, 8):
                 x_copy(q, kind).wait_send()
 
         for k in range(2):
@@ -678,6 +725,31 @@
         return carry
 
     lax.fori_loop(0, nz, drain, 0)
+
+
+def hand_kernel(a_in, b_in, a_out, b_out, sem):
+    copies = [
+        pltpu.make_async_copy(a_in, a_out, sem.at[0]),
+        pltpu.make_async_copy(b_in, b_out, sem.at[1]),
+    ]
+    for copy in copies:
+        copy.start()
+    for copy in copies:
+        copy.wait()
+
+
+def hand_over(a, b):
+    hbm = pl.BlockSpec(memory_space=pltpu.HBM)
+    vmem = pl.BlockSpec(memory_space=pltpu.VMEM)
+    return pl.pallas_call(
+        hand_kernel,
+        out_shape=tuple(jax.ShapeDtypeStruct(v.shape, v.dtype) for v in (a, b)),
+        in_specs=[vmem, vmem],
+        out_specs=(hbm, hbm),
+        scratch_shapes=[pltpu.SemaphoreType.DMA((2,))],
+        compiler_params=pltpu.CompilerParams(vmem_limit_bytes=4 << 20),
+        name="hand",
+    )(a, b)
 
 
 def both_fused(
@@ -710,19 +782,16 @@
     hbm = pl.BlockSpec(memory_space=pltpu.HBM)
     dma = pltpu.SemaphoreType.DMA
     flops = 2 * n_ep * cap * features * (2 * ff_dev + out_dev)
-    return pl.pallas_call(
+    results = pl.pallas_call(
         functools.partial(both_kernel, cap),
-        out_shape=(
-            jax.ShapeDtypeStruct((rows, width), BF16),
-            jax.ShapeDtypeStruct((rows, out_dev), BF16),
-        ),
+        out_shape=(pltpu.VMEM((rows, width), BF16), pltpu.VMEM((rows, out_dev), BF16)),
         in_specs=[hbm] * 6 + [vmem] * 3 + [hbm] + [vmem] * 3 + [hbm] * 3,
         out_specs=(vmem, vmem),
         scratch_shapes=[
             pltpu.VMEM((rows, features), BF16),
-            pltpu.VMEM((nz, 2, rows, share), BF16),
+            pltpu.VMEM((nz, 4, rows, share), BF16),
             pltpu.VMEM((nz, pair, features), BF16),
-            pltpu.VMEM((nz, 2, cap, share), BF16),
+            pltpu.VMEM((nz, 4, cap, share), BF16),
             pltpu.VMEM((cap, features), BF16),
             pltpu.VMEM((nz, pair, rows), BF16),
             pltpu.VMEM((nz, pair, 2 * ff_dev), BF16),
@@ -740,11 +809,11 @@
             pltpu.VMEM((2, 2 * ff_dev, out_dev), BF16),
             dma((11,)),
             dma((2, nz)),
-            dma((2, 2, nz)),
-            dma((2, nz)),
+            dma((2, 4, nz)),
+            dma((4, nz)),
             dma((2, 4)),
-            dma((6, nz)),
-            dma((6, nz)),
+            dma((8, nz)),
+            dma((8, nz)),
             dma((2, n_ep)),
             dma((2, n_ep)),
             dma((2, n_ep)),
@@ -763,7 +832,7 @@
             dma((2, n_ep)),
         ],
         compiler_params=pltpu.CompilerParams(
-            collective_id=0, has_side_effects=True, vmem_limit_bytes=60 * 1024 * 1024
+            collective_id=0, has_side_effects=True, vmem_limit_bytes=66000000
         ),
         cost_estimate=pl.CostEstimate(flops=flops, bytes_accessed=16 << 20, transcendentals=0),
         name="both",
@@ -785,6 +854,7 @@
         expert_up,
         expert_down,
     )
+    return hand_over(*results)
 
 
 def from_behind(value, axis, by):

time: 80.1 us -> 72.9 us (0.910)
  Pallas kernels: 75.9 us -> 71.9 us
  local copies, waits for them, and re-layouts: 3.34 us -> 0 us
    pallas_call x1 -> x2, Pallas kernels: 75.9 us -> 71.9 us  [the longest x1 71.1 us: both_fused(): pl.pallas_call(functools.partial(both_kernel, cap), out_shape=(pltpu.VMEM...]
    unnamed x2 -> x0, local copies, waits for them, and re-layouts: 3.34 us -> none
where the time goes in v2:
time: 72.9 us; the launch traced here: 72.6 us
  Pallas kernels  71.9 us (99%)
    pallas_call x1, Pallas kernels, both_fused(): pl.pallas_call(functools.partial(both_kernel, cap), out_shape=(pltpu.VMEM...  71.1 us

profile of v2, /device:TPU:1, one launch (start us, length us, event | category | flops | bytes accessed | tf_op | source)
XLA Modules:
  0.0 72.6 jit_solution(5281301070399568267)
XLA Ops:
  0.6 71.1 %both.1 = (bf16[256,512]{1,0:T(8,128)(2,1)S(1)}, bf16[256,512]{1,0:T(8,128)(2,1)S(1)}) custom-call(bf16[256,2048]{1,0:T(8,128)(2,1)} %mix_hbm.1, bf16[2048,512]{1,0:T(8,128)(2,1)} %wx_hbm.1, bf16[2048,512]{1,0:T(8,128)(2,1)} %wy_hbm.1, bf16[4,128,128]{2,1,0:T(8,128)(2,1)} %ga_hbm.1, bf16[4,128,128]{2,1,0:T(8,128)(2,1)} %gx_hbm.1, f32[256,512]{1,0:T(8,128)} %shift_hbm.1, ...), custom_call_target="tpu_custom_call" | custom-call | flops 6442450944 | bytes 16777216 | tf_op jit(solution)/shard_map/both/pallas_call | solution.py:785
  71.8 0.8 %hand.1 = (bf16[256,512]{1,0:T(8,128)(2,1)}, bf16[256,512]{1,0:T(8,128)(2,1)}) custom-call(bf16[256,512]{1,0:T(8,128)(2,1)S(1)} %get-tuple-element.4.a_in, bf16[256,512]{1,0:T(8,128)(2,1)S(1)} %get-tuple-element.5.b_in), custom_call_target="tpu_custom_call" | custom-call | tf_op jit(solution)/shard_map/hand/pallas_call | solution.py:744

commit v3 on v2

--- a/solution.py
+++ b/solution.py
@@ -42,18 +42,25 @@
     ga_hbm,
     gx_hbm,
     shift_hbm,
-    mix_gain_ref,
-    taps_ref,
-    logit_ref,
+    mix_gain_hbm,
+    taps_hbm,
+    logit_hbm,
     moe_hbm,
-    gain_ref,
-    rt_row,
-    rw_row,
+    gain_hbm,
+    rt_hbm,
+    rw_hbm,
     gate_hbm,
     up_hbm,
     down_hbm,
     mix_ref,
     out_ref,
+    mix_gain_ref,
+    taps_ref,
+    logit_ref,
+    gain_ref,
+    rt_row,
+    rw_row,
+    small_sem,
     nrm,
     tok,
     xs,
@@ -80,6 +87,7 @@
     w_sem,
     x_send,
     x_recv,
+    push_sem,
     ag_sem,
     rs_sem,
     ret_sem,
@@ -146,7 +154,17 @@
         pltpu.make_async_copy(down_rows(t), w2.at[0, pl.ds(0, half)], load_sem.at[9]),
         pltpu.make_async_copy(down_rows(pa), w2.at[0, pl.ds(half, half)], load_sem.at[10]),
     ]
+    small = [
+        pltpu.make_async_copy(gain_hbm, gain_ref, small_sem.at[0]),
+        pltpu.make_async_copy(rt_hbm, rt_row, small_sem.at[1]),
+        pltpu.make_async_copy(rw_hbm, rw_row, small_sem.at[2]),
+        pltpu.make_async_copy(mix_gain_hbm, mix_gain_ref, small_sem.at[3]),
+        pltpu.make_async_copy(taps_hbm, taps_ref, small_sem.at[4]),
+        pltpu.make_async_copy(logit_hbm, logit_ref, small_sem.at[5]),
+    ]
     loads[0].start()
+    for copy in small[:2]:
+        copy.start()
     barrier = pltpu.get_barrier_semaphore()
     for by in range(1, n_ep):
         pl.semaphore_signal(
@@ -157,18 +175,21 @@
             pl.semaphore_signal(
                 barrier, inc=1, device_id={"ep": near, "tp": peer}, device_id_type=MESH
             )
-    for copy in loads[3:6] + loads[1:3] + loads[6:]:
+    for copy in small[2:] + loads[3:6] + loads[1:3] + loads[6:]:
         copy.start()
 
     def columns(k):
         return pl.ds(pl.multiple_of(k * share, share), share)
+
+    def z_slot(q, k):
+        return q * 2 + k if k < 2 else nz * 2 + k - 2
 
     def z_own(k, up):
         return remote(
             nrm.at[:, columns(shares[k])],
             tok.at[z, k],
-            z_send.at[up, k, z],
-            z_recv.at[k, z],
+            z_send.at[z],
+            z_recv.at[z_slot(z, k)],
             {"ep": ep + (2 if up else -2)},
         )
 
@@ -176,13 +197,13 @@
         return remote(
             tok.at[q, k],
             tok.at[q, k],
-            z_send.at[up, k, q],
-            z_recv.at[k, q],
+            z_send.at[q],
+            z_recv.at[z_slot(q, k)],
             {"ep": ep + (2 if up else -2)},
         )
 
     def route_copy(q):
-        return remote(rt_row, routes_all.at[z], rt_sem.at[0, q], rt_sem.at[1, z], {"ep": q * 2 + c})
+        return remote(rt_row, routes_all.at[z], rt_sem.at[nz], rt_sem.at[z], {"ep": q * 2 + c})
 
     def w_copy(k):
         piece = half // 2
@@ -190,8 +211,8 @@
         return remote(
             down_hbm.at[0, pl.ds(pl.multiple_of(first, piece), piece)],
             w2.at[1, pl.ds(k * piece, piece)],
-            w_sem.at[0, k],
-            w_sem.at[1, k],
+            w_sem.at[0],
+            w_sem.at[1],
             {"tp": pb},
         )
 
@@ -205,24 +226,21 @@
         return remote(
             src,
             xs_part(q, c, shares[max(kind - 4, 0)]),
-            x_send.at[kind, q],
-            x_recv.at[kind, q],
+            x_send.at[q],
+            x_recv.at[q],
             {"ep": near, "tp": to},
         )
 
-    def x_wait(q, kind):
-        block = c if kind < 2 else 1 - c
-        dst = xs_part(q, block, (xp, yp, xp, yp, t, dg, xp, yp)[kind])
-        remote(
-            stage.at[q, 0], dst, x_send.at[kind, q], x_recv.at[kind, q], {"ep": other}
-        ).wait_recv()
+    def x_all(q, count):
+        part = xs.at[q, pl.ds(0, count * cap // 4)]
+        return remote(part, part, x_send.at[q], x_recv.at[q], {"ep": other})
 
     def own_copy(block):
         return remote(
             own_stage,
             xs.at[z, pl.ds(pl.multiple_of(block * cap, cap), cap)],
-            x_send.at[4, z],
-            x_recv.at[4, z],
+            x_send.at[z],
+            x_recv.at[z],
             {"ep": other},
         )
 
@@ -231,23 +249,23 @@
         return remote(
             hid.at[q, at, pl.ds(0, half)],
             hid.at[q, at, pl.ds(half, half)],
-            ag_sem.at[0, sem],
-            ag_sem.at[1, sem],
+            push_sem.at[0],
+            ag_sem.at[sem],
             {"tp": pa},
         )
 
     def rs_copy(q, cc):
         at, sem = pl.ds(cc * cap, cap), q * 2 + cc
         return remote(
-            psend.at[q, at], precv.at[q, at], rs_sem.at[0, sem], rs_sem.at[1, sem], {"tp": pb}
+            psend.at[q, at], precv.at[q, at], push_sem.at[0], rs_sem.at[sem], {"tp": pb}
         )
 
     def ret_copy(q, cc):
         return remote(
             res.at[q, pl.ds(cc * cap, cap)],
             ret.at[ep],
-            ret_sem.at[0, q * 2 + cc],
-            ret_sem.at[1, ep],
+            push_sem.at[1],
+            ret_sem.at[ep],
             {"ep": q * 2 + cc},
         )
 
@@ -306,9 +324,8 @@
             u = jnp.dot(xs[q], uw[:, cols], preferred_element_type=F32)
             hid[q, :, cols] = (jax.nn.silu(g) * u).astype(BF16)
 
-    def gathered(q, kinds=range(6)):
-        for kind in kinds:
-            x_wait(q, kind)
+    def gathered(q, count=6):
+        x_all(q, count).wait_recv()
 
     def ag_start(q):
         for cc in range(2):
@@ -367,10 +384,14 @@
         return remote(
             ends.at[ep],
             ends.at[ep],
-            ends_sem.at[0, by],
-            ends_sem.at[1, ep],
+            ends_sem.at[0],
+            ends_sem.at[1],
             {"ep": (ep + by) % n_ep},
         )
+
+    def ends_all():
+        part = ends.at[pl.ds(0, n_ep - 1)]
+        return remote(part, part, ends_sem.at[0], ends_sem.at[1], {"ep": other})
 
     def norm(buffer, gain):
         strip = 64
@@ -463,11 +484,7 @@
 
     def finish():
         carried = jnp.zeros((1, av.shape[1]), F32)
-        for by in range(1, n_ep):
-            peer = (ep + by) % n_ep
-            remote(
-                ends.at[peer], ends.at[peer], ends_sem.at[0, 0], ends_sem.at[1, peer], {"ep": peer}
-            ).wait_recv()
+        ends_all().wait_recv()
         for k in range(n_ep):
             entered = ends[k, 0:1] * carried + ends[k, 1:2]
             carried = jnp.where(k < ep, entered, carried)
@@ -478,6 +495,39 @@
             at = pl.ds(pl.multiple_of(i * strip, strip), strip)
             state = bv[at, :] + av[at, :] * carried
             mix_ref[at, :] = (state * jax.nn.gelu(yb[at, :].astype(F32))).astype(BF16)
+
+    def drain_early():
+        part = xs.at[0]
+        remote(part, part, z_send.at[z], z_recv.at[0], {"ep": other}).wait_send()
+        remote(part, part, w_sem.at[0], w_sem.at[1], {"ep": other}).wait_send()
+        own_copy(c).wait_send()
+        ends_all().wait_send()
+        part = routes_all.at[pl.ds(0, nz - 1)]
+        remote(part, part, rt_sem.at[nz], rt_sem.at[0], {"ep": other}).wait_send()
+
+        @pl.when(ep + 1 < n_ep)
+        def _():
+            halo_copy().wait_send()
+
+        def drain_one(q, carry):
+            whole = inner & (q == block_at(2))
+
+            @pl.when((q != z) & jnp.logical_not(whole))
+            def _():
+                x_all(q, 6).wait_send()
+
+            @pl.when(whole)
+            def _():
+                x_all(q, 4).wait_send()
+
+            @pl.when((q != z) & inner)
+            def _():
+                part = tok.at[q, pl.ds(0, 2)]
+                remote(part, part, z_send.at[q], z_recv.at[0], {"ep": other}).wait_send()
+
+            return carry
+
+        lax.fori_loop(0, nz, drain_one, 0)
 
     def make_combine():
         weights = rw_row[...]
@@ -523,7 +573,7 @@
 
     def ret_wait(e):
         remote(
-            res.at[0, pl.ds(0, cap)], ret.at[e], ret_sem.at[0, 0], ret_sem.at[1, e], {"ep": other}
+            res.at[0, pl.ds(0, cap)], ret.at[e], push_sem.at[1], ret_sem.at[e], {"ep": other}
         ).wait_recv()
 
     def combine_far(e, first=False, last=False):
@@ -531,6 +581,8 @@
         combine(e, ret[e], first, last)
 
     loads[0].wait()
+    for copy in small[:2]:
+        copy.wait()
     norm(nrm, gain_ref)
     pl.semaphore_wait(barrier, n_ep + 3)
     for q in range(nz):
@@ -553,10 +605,12 @@
         w_copy(k).start()
     make_picks(z, rt_row[...])
     pick_own()
+    for copy in small[2:]:
+        copy.wait()
     one, two, three = block_at(0), block_at(1), block_at(2)
     for q in (one, two, three):
         remote(
-            rt_row, routes_all.at[q], rt_sem.at[0, 0], rt_sem.at[1, q], {"ep": q * 2 + c}
+            rt_row, routes_all.at[q], rt_sem.at[nz], rt_sem.at[q], {"ep": q * 2 + c}
         ).wait_recv()
         make_picks(q, routes_all[q])
     project()
@@ -587,8 +641,7 @@
     pick(two, 0)
     for k in range(9, 11):
         loads[k].wait()
-    for k in range(4):
-        w_copy(k).wait_recv()
+    remote(w2.at[1], w2.at[1], w_sem.at[0], w_sem.at[1], {"tp": pb}).wait_recv()
     down_other(one, 0)
     down_other(one, 1)
     down_own(one)
@@ -636,7 +689,7 @@
 
     @pl.when(inner)
     def _():
-        gathered(three, range(4, 8))
+        gathered(three, 4)
 
     gate_up(three)
     ag_start(three)
@@ -657,74 +710,15 @@
     combine_far(one * 2 + 1)
     give_own()
     combine(ep, res[z, pl.ds(pl.multiple_of(c * cap, cap), cap)])
+    drain_early()
     combine_far(other)
     combine_far(three * 2 + 0)
     combine_far(three * 2 + 1, last=True)
 
-    for k in range(4):
-
-        @pl.when((z + 1 < nz) & ((z == 0) | (k < 2)))
-        def _():
-            z_own(k, 1).wait_send()
-
-        @pl.when((z > 0) & ((z + 1 == nz) | (k < 2)))
-        def _():
-            z_own(k, 0).wait_send()
-
-    for k in range(4):
-        w_copy(k).wait_send()
-
-    own_copy(c).wait_send()
-
-    @pl.when(ep + 1 < n_ep)
-    def _():
-        halo_copy().wait_send()
-
-    for by in range(1, n_ep):
-        ends_copy(by).wait_send()
-
-    def drain(q, carry):
-        for cc in range(2):
-            ag_copy(q, cc).wait_send()
-            rs_copy(q, cc).wait_send()
-
-        @pl.when(q != z)
-        def _():
-            route_copy(q).wait_send()
-            for kind in range(4, 6):
-                x_copy(q, kind).wait_send()
-
-        whole = inner & (q == block_at(2))
-
-        @pl.when((q != z) & jnp.logical_not(whole))
-        def _():
-            for kind in range(4):
-                x_copy(q, kind).wait_send()
-
-        @pl.when(whole)
-        def _():
-            for kind in range(6, 8):
-                x_copy(q, kind).wait_send()
-
-        for k in range(2):
-
-            @pl.when((q < z) & (z + 1 < nz))
-            def _():
-                z_copy(q, k, 1).wait_send()
-
-            @pl.when((q > z) & (z > 0))
-            def _():
-                z_copy(q, k, 0).wait_send()
-
-        for cc in range(2):
-
-            @pl.when((q != z) | (c != cc))
-            def _():
-                ret_copy(q, cc).wait_send()
-
-        return carry
-
-    lax.fori_loop(0, nz, drain, 0)
+    part = xs.at[pl.ds(0, 2)]
+    remote(part, part, push_sem.at[0], ag_sem.at[0], {"ep": other}).wait_send()
+    part = xs.at[0, pl.ds(0, (n_ep - 1) * cap // 4)]
+    remote(part, part, push_sem.at[1], ag_sem.at[0], {"ep": other}).wait_send()
 
 
 def hand_kernel(a_in, b_in, a_out, b_out, sem):
@@ -785,9 +779,16 @@
     results = pl.pallas_call(
         functools.partial(both_kernel, cap),
         out_shape=(pltpu.VMEM((rows, width), BF16), pltpu.VMEM((rows, out_dev), BF16)),
-        in_specs=[hbm] * 6 + [vmem] * 3 + [hbm] + [vmem] * 3 + [hbm] * 3,
+        in_specs=[hbm] * 16,
         out_specs=(vmem, vmem),
         scratch_shapes=[
+            pltpu.VMEM((1, features), F32),
+            pltpu.VMEM(conv_taps.shape, F32),
+            pltpu.VMEM((1, width), F32),
+            pltpu.VMEM((1, features), F32),
+            pltpu.VMEM(routes.shape[::-1], jnp.int32),
+            pltpu.VMEM(routes.shape[::-1], F32),
+            dma((6,)),
             pltpu.VMEM((rows, features), BF16),
             pltpu.VMEM((nz, 4, rows, share), BF16),
             pltpu.VMEM((nz, pair, features), BF16),
@@ -808,15 +809,16 @@
             pltpu.VMEM(expert_up.shape[1:], BF16),
             pltpu.VMEM((2, 2 * ff_dev, out_dev), BF16),
             dma((11,)),
-            dma((2, nz)),
-            dma((2, 4, nz)),
-            dma((4, nz)),
-            dma((2, 4)),
-            dma((8, nz)),
-            dma((8, nz)),
-            dma((2, n_ep)),
-            dma((2, n_ep)),
-            dma((2, n_ep)),
+            dma((nz + 1,)),
+            dma((nz,)),
+            dma((2 * nz + 2,)),
+            dma((2,)),
+            dma((nz,)),
+            dma((nz,)),
+            dma((2,)),
+            dma((n_ep,)),
+            dma((n_ep,)),
+            dma((n_ep,)),
             pltpu.VMEM(mix_in.shape, BF16),
             pltpu.VMEM(w_in_x.shape, BF16),
             pltpu.VMEM(w_in_y.shape, BF16),
@@ -829,7 +831,7 @@
             pltpu.VMEM((rows, width), F32),
             pltpu.VMEM((n_ep, 2, width), F32),
             dma((2,)),
-            dma((2, n_ep)),
+            dma((2,)),
         ],
         compiler_params=pltpu.CompilerParams(
             collective_id=0, has_side_effects=True, vmem_limit_bytes=66000000

time: 72.9 us -> 71.1 us (0.975)
  Pallas kernels: 71.9 us -> 70 us
    pallas_call x1, Pallas kernels: 71.1 us -> 69.1 us  [both_fused(): pl.pallas_call(functools.partial(both_kernel, cap), out_shape=(pltpu.VMEM...]
where the time goes in v3:
time: 71.1 us; the launch traced here: 70.6 us
  Pallas kernels  70 us (98%)
    pallas_call x1, Pallas kernels, both_fused(): pl.pallas_call(functools.partial(both_kernel, cap), out_shape=(pltpu.VMEM...  69.1 us

profile of v3, /device:TPU:1, one launch (start us, length us, event | category | flops | bytes accessed | tf_op | source)
XLA Modules:
  0.0 70.6 jit_solution(12089397408191320487)
XLA Ops:
  0.6 69.1 %both.1 = (bf16[256,512]{1,0:T(8,128)(2,1)S(1)}, bf16[256,512]{1,0:T(8,128)(2,1)S(1)}) custom-call(bf16[256,2048]{1,0:T(8,128)(2,1)} %mix_hbm.1, bf16[2048,512]{1,0:T(8,128)(2,1)} %wx_hbm.1, bf16[2048,512]{1,0:T(8,128)(2,1)} %wy_hbm.1, bf16[4,128,128]{2,1,0:T(8,128)(2,1)} %ga_hbm.1, bf16[4,128,128]{2,1,0:T(8,128)(2,1)} %gx_hbm.1, f32[256,512]{1,0:T(8,128)} %shift_hbm.1, ...), custom_call_target="tpu_custom_call" | custom-call | flops 6442450944 | bytes 16777216 | tf_op jit(solution)/shard_map/both/pallas_call | solution.py:779
  69.8 0.8 %hand.1 = (bf16[256,512]{1,0:T(8,128)(2,1)}, bf16[256,512]{1,0:T(8,128)(2,1)}) custom-call(bf16[256,512]{1,0:T(8,128)(2,1)S(1)} %get-tuple-element.4.a_in, bf16[256,512]{1,0:T(8,128)(2,1)S(1)} %get-tuple-element.5.b_in), custom_call_target="tpu_custom_call" | custom-call | tf_op jit(solution)/shard_map/hand/pallas_call | solution.py:738

commit v4 on v3

--- a/solution.py
+++ b/solution.py
@@ -315,7 +315,7 @@
             x_copy(q, kind).start()
 
     def gate_up(q):
-        tile = 256
+        tile = 512
 
         @pl.loop(0, gw.shape[1] // tile)
         def _(j):
@@ -332,7 +332,7 @@
             ag_copy(q, cc).start()
 
     def down_other(q, cc):
-        tile = 256
+        tile = 512
         at = pl.ds(cc * cap, cap)
         ag_copy(q, cc).wait_recv()
 
@@ -346,7 +346,7 @@
         rs_copy(q, cc).start()
 
     def down_own(q):
-        tile = 256
+        tile = 512
 
         @pl.loop(0, span // tile)
         def _(j):
@@ -699,19 +699,19 @@
     down_other(three, 0)
     down_other(three, 1)
     down_own(three)
+    down_other(z, 0)
     give(three, 0)
+    down_other(z, 1)
     give(three, 1)
-    down_other(z, 0)
-    down_other(z, 1)
     down_own(z)
+    give_own()
     combine_far(two * 2 + 0, first=True)
     combine_far(two * 2 + 1)
+    combine(ep, res[z, pl.ds(pl.multiple_of(c * cap, cap), cap)])
+    combine_far(other)
+    drain_early()
     combine_far(one * 2 + 0)
     combine_far(one * 2 + 1)
-    give_own()
-    combine(ep, res[z, pl.ds(pl.multiple_of(c * cap, cap), cap)])
-    drain_early()
-    combine_far(other)
     combine_far(three * 2 + 0)
     combine_far(three * 2 + 1, last=True)
 

time: 71.1 us -> 70.1 us (0.986)
  Pallas kernels: 70 us -> 69.1 us
    pallas_call x1, Pallas kernels: 69.1 us -> 68.3 us  [both_fused(): pl.pallas_call(functools.partial(both_kernel, cap), out_shape=(pltpu.VMEM...]
where the time goes in v4:
time: 70.1 us; the launch traced here: 69.9 us
  Pallas kernels  69.1 us (99%)
  between operations  0.81 us (1%)
    pallas_call x1, Pallas kernels, both_fused(): pl.pallas_call(functools.partial(both_kernel, cap), out_shape=(pltpu.VMEM...  68.3 us

profile of v4, /device:TPU:1, one launch (start us, length us, event | category | flops | bytes accessed | tf_op | source)
XLA Modules:
  0.0 69.9 jit_solution(6969707897115012169)
XLA Ops:
  0.6 68.3 %both.1 = (bf16[256,512]{1,0:T(8,128)(2,1)S(1)}, bf16[256,512]{1,0:T(8,128)(2,1)S(1)}) custom-call(bf16[256,2048]{1,0:T(8,128)(2,1)} %mix_hbm.1, bf16[2048,512]{1,0:T(8,128)(2,1)} %wx_hbm.1, bf16[2048,512]{1,0:T(8,128)(2,1)} %wy_hbm.1, bf16[4,128,128]{2,1,0:T(8,128)(2,1)} %ga_hbm.1, bf16[4,128,128]{2,1,0:T(8,128)(2,1)} %gx_hbm.1, f32[256,512]{1,0:T(8,128)} %shift_hbm.1, ...), custom_call_target="tpu_custom_call" | custom-call | flops 6442450944 | bytes 16777216 | tf_op jit(solution)/shard_map/both/pallas_call | solution.py:779
  69.0 0.8 %hand.1 = (bf16[256,512]{1,0:T(8,128)(2,1)}, bf16[256,512]{1,0:T(8,128)(2,1)}) custom-call(bf16[256,512]{1,0:T(8,128)(2,1)S(1)} %get-tuple-element.4.a_in, bf16[256,512]{1,0:T(8,128)(2,1)S(1)} %get-tuple-element.5.b_in), custom_call_target="tpu_custom_call" | custom-call | tf_op jit(solution)/shard_map/hand/pallas_call | solution.py:738

commit v5 on v4

--- a/solution.py
+++ b/solution.py
@@ -162,7 +162,17 @@
         pltpu.make_async_copy(taps_hbm, taps_ref, small_sem.at[4]),
         pltpu.make_async_copy(logit_hbm, logit_ref, small_sem.at[5]),
     ]
-    loads[0].start()
+    strip_rows = rows // 4
+    strips = [
+        pltpu.make_async_copy(
+            moe_hbm.at[pl.ds(i * strip_rows, strip_rows)],
+            nrm.at[pl.ds(i * strip_rows, strip_rows)],
+            load_sem.at[0 if i == 0 else 10 + i],
+        )
+        for i in range(4)
+    ]
+    for copy in strips:
+        copy.start()
     for copy in small[:2]:
         copy.start()
     barrier = pltpu.get_barrier_semaphore()
@@ -580,10 +590,14 @@
         ret_wait(e)
         combine(e, ret[e], first, last)
 
-    loads[0].wait()
     for copy in small[:2]:
         copy.wait()
-    norm(nrm, gain_ref)
+    for i in range(4):
+        strips[i].wait()
+        at = pl.ds(i * strip_rows, strip_rows)
+        wide = nrm[at, :].astype(F32)
+        scale = lax.rsqrt(jnp.mean(wide * wide, axis=-1, keepdims=True) + epsilon)
+        nrm[at, :] = (wide * scale * gain_ref[...]).astype(BF16)
     pl.semaphore_wait(barrier, n_ep + 3)
     for q in range(nz):
 
@@ -808,7 +822,7 @@
             pltpu.VMEM(expert_gate.shape[1:], BF16),
             pltpu.VMEM(expert_up.shape[1:], BF16),
             pltpu.VMEM((2, 2 * ff_dev, out_dev), BF16),
-            dma((11,)),
+            dma((14,)),
             dma((nz + 1,)),
             dma((nz,)),
             dma((2 * nz + 2,)),

time: 70.1 us -> 69.8 us (level)
  no operation moved by 1% of the time
where the time goes in v5:
time: 69.8 us; the launch traced here: 69.7 us
  Pallas kernels  68.9 us (99%)
  between operations  0.81 us (1%)
    pallas_call x1, Pallas kernels, both_fused(): pl.pallas_call(functools.partial(both_kernel, cap), out_shape=(pltpu.VMEM...  68.1 us

profile of v5, /device:TPU:1, one launch (start us, length us, event | category | flops | bytes accessed | tf_op | source)
XLA Modules:
  0.0 69.7 jit_solution(15101916832745039328)
XLA Ops:
  0.6 68.1 %both.1 = (bf16[256,512]{1,0:T(8,128)(2,1)S(1)}, bf16[256,512]{1,0:T(8,128)(2,1)S(1)}) custom-call(bf16[256,2048]{1,0:T(8,128)(2,1)} %mix_hbm.1, bf16[2048,512]{1,0:T(8,128)(2,1)} %wx_hbm.1, bf16[2048,512]{1,0:T(8,128)(2,1)} %wy_hbm.1, bf16[4,128,128]{2,1,0:T(8,128)(2,1)} %ga_hbm.1, bf16[4,128,128]{2,1,0:T(8,128)(2,1)} %gx_hbm.1, f32[256,512]{1,0:T(8,128)} %shift_hbm.1, ...), custom_call_target="tpu_custom_call" | custom-call | flops 6442450944 | bytes 16777216 | tf_op jit(solution)/shard_map/both/pallas_call | solution.py:793
  68.7 0.8 %hand.1 = (bf16[256,512]{1,0:T(8,128)(2,1)}, bf16[256,512]{1,0:T(8,128)(2,1)}) custom-call(bf16[256,512]{1,0:T(8,128)(2,1)S(1)} %get-tuple-element.4.a_in, bf16[256,512]{1,0:T(8,128)(2,1)S(1)} %get-tuple-element.5.b_in), custom_call_target="tpu_custom_call" | custom-call | tf_op jit(solution)/shard_map/hand/pallas_call | solution.py:752
